TPU v7x, 512 devices: a whole 4x4x16 slice. The times are simulated.
512 devices in a mesh: sp: 64 (over z, y), tp: 8 (over x, core).
Axes of the slice: x: 4, y: 4, z: 16, core: 2. Of those that a mesh axis runs over, the one named last changes fastest.
Arguments:
- tokens: bfloat16 [16384, 2048], P('sp'), may hold values from -6 to 6
- input_norm_gain: float32 [2048], replicated, may hold values from 0.1 to 1.9
- query_matrix: bfloat16 [2048, 1024], P('sp', 'tp'), may hold values from -0.125 to 0.125
- key_matrix: bfloat16 [2048, 1024], P('sp', 'tp'), may hold values from -0.125 to 0.125
- value_matrix: bfloat16 [2048, 1024], P('sp', 'tp'), may hold values from -0.125 to 0.125
- convolution_value_matrix: bfloat16 [2048, 2048], P('sp', 'tp'), may hold values from -0.125 to 0.125
- convolution_gate_matrix: bfloat16 [2048, 2048], P('sp', 'tp'), may hold values from -0.125 to 0.125
- decay_offset_channel: float32 [1024], P('tp'), may hold values from -16 to -2
- decay_first_matrix: bfloat16 [2048, 128], replicated, may hold values from -0.125 to 0.125
- decay_second_matrix: bfloat16 [128, 1024], P(None, 'tp'), may hold values from -0.59765625 to 0.59765625
- learning_rate_offset: float32 [1024], P('tp'), may hold values from -9 to 1
- learning_rate_first_matrix: bfloat16 [2048, 128], replicated, may hold values from -0.125 to 0.125
- learning_rate_second_matrix: bfloat16 [128, 1024], P(None, 'tp'), may hold values from -0.5 to 0.5
- forgetting_rate_factor: float32 [16384, 16], P('sp', 'tp'), may hold values from 0.39 to 2.53
- state_retention_share: float32 [16384, 16], P('sp', 'tp'), may hold values from 0.12 to 1
- per_head_norm_gain: float32 [1024], P('tp'), may hold values from 0.1 to 1.9
- convolution_filter_taps: float32 [31, 2048], P(None, 'tp'), may hold values from -81 to 81
- convolution_channel_gain: float32 [2048], P('tp'), may hold values from 0.1 to 1.9
- attention_output_matrix: bfloat16 [2048, 1024], P('sp', 'tp'), may hold values from -0.109375 to 0.109375
- convolution_output_matrix: bfloat16 [2048, 2048], P('sp', 'tp'), may hold values from -0.109375 to 0.109375
Outputs:
- mixed: bfloat16 [16384, 2048], P('sp')
All inputs are finite; a program needn't handle non-finite values.
Results may differ from a plain program's by a relative error of at most 0.014.
Values may be sent and summed in bfloat16 or wider, within the bound.
No kernel may reach another device: no remote copies, remote signals or barrier semaphores. Data moves between devices by JAX's collectives and lax.ppermute only.
A program may use at most 64 MiB of HBM per device.

v0:
```python
import math

import jax
import jax.numpy as jnp
from jax import lax
from jax.sharding import Mesh
from jax.sharding import PartitionSpec as P

CONV_CH = 2048
SP = ("sp_0", "sp_1")


HIGHEST = lax.Precision.HIGHEST
RMS_EPSILON = 1e-06
GROUP_EPSILON = 0.00064
LAYER_EPSILON = 1e-05
UNIT_EPSILON = 1e-06


def in_one_piece(arrays, axis, dim, along):
    widths = [a.shape[along] for a in arrays]
    both = jnp.concatenate(arrays, axis=along)
    out = lax.all_gather(both, axis, axis=dim, tiled=True)
    return tuple(jnp.split(out, [sum(widths[:k]) for k in range(1, len(widths))], axis=along))


def nothing_yet(x, identity):
    return jax.tree.map(
        lambda a, e: jnp.broadcast_to(jnp.asarray(e, a.dtype), a.shape), x, identity
    )


def collected_together(x, axis):
    leaves = jax.tree.leaves(x)
    turns = sorted(range(len(leaves)), key=lambda k: -leaves[k].size)
    width = (1, *leaves[turns[0]].shape)[-1]
    lines = [
        jnp.pad(leaves[k].reshape(-1), (0, -leaves[k].size % width)).reshape(-1, width)
        for k in turns
    ]
    both, at, found = (lax.all_gather(jnp.concatenate(lines), axis), 0, {})
    for k, line in zip(turns, lines):
        piece = both[:, at : at + len(line)].reshape(len(both), -1)
        found[k] = piece[:, : leaves[k].size].reshape(-1, *leaves[k].shape)
        at += len(line)
    numbers = iter(range(len(leaves)))
    return jax.tree.map(lambda _: found[next(numbers)], x)


def prefix_by_axis(x, axes, combine, identity):
    before = start = nothing_yet(x, identity)
    so_far = x
    for axis in reversed(axes):
        count, place = (lax.axis_size(axis), lax.axis_index(axis))
        pieces = collected_together(so_far, axis)
        inside, so_far = (start, start)
        for k in range(count):
            passed = k < place
            so_far = combine(so_far, jax.tree.map(lambda part: part[k], pieces))
            inside = jax.tree.map(lambda new, old: jnp.where(passed, new, old), so_far, inside)
        before = combine(inside, before)
    return before


def from_behind(value, axis, steps):
    count = lax.axis_size(axis)
    initial, last = (max(0, -steps), min(count, count - steps))
    return lax.ppermute(value, axis, [(source, source + steps) for source in range(initial, last)])


def from_everyone(x, axis):
    copies = jnp.broadcast_to(x, (lax.axis_size(axis), *x.shape))
    return lax.all_to_all(copies, axis, split_axis=0, concat_axis=0, tiled=True)


def in_order(parts, dim):
    parts = jnp.moveaxis(parts, 0, dim)
    lengths = parts.shape
    return parts.reshape(*lengths[:dim], lengths[dim] * lengths[dim + 1], *lengths[dim + 2 :])


def gathered_copies(x, axis, dim):
    parts = from_everyone(x, axis)
    return in_order(parts, dim)


def sent_together(arrays, axis, dim, along):
    ends, at = ([], 0)
    for a in arrays[:-1]:
        at += a.shape[along]
        ends.append(at)
    both = jnp.concatenate(arrays, axis=along)
    return tuple(jnp.split(gathered_copies(both, axis, dim), ends, axis=along))


def total_of_pieces(x, axis):
    return lax.all_gather(x, axis).astype(jnp.float32).sum(0)


def exact_mul(form, left, right):
    return jnp.einsum(form, left, right, precision=HIGHEST)


def chain_pair(earlier, later):
    return (
        exact_mul("...cd,...de->...ce", earlier[0], later[0]),
        exact_mul("...vd,...de->...ve", earlier[1], later[0]) + later[1],
    )


def split_blocks(values, block_count, block_len):
    return values.reshape((block_count, block_len) + values.shape[1:]).transpose(0, 2, 1, 3)


def block_update(carry, inputs):
    phi_sofar, psi_sofar = carry
    query_blk, logdec_blk, key_blk, value_blk, erase_blk, write_blk = inputs
    block_len = query_blk.shape[1]
    head_size = query_blk.shape[2]
    log_gain = jnp.cumsum(logdec_blk, axis=1)
    log_before = log_gain - logdec_blk
    positions = jnp.arange(block_len)
    strict = positions[:, None] > positions[None, :]
    pair_decay = jnp.exp(
        jnp.where(
            strict[None, :, :, None], log_before[:, :, None, :] - log_gain[:, None, :, :], -jnp.inf
        )
    )

    def paired(left, right):
        return jnp.einsum("htc,htsc,hsc->hts", left, pair_decay, right, precision=HIGHEST)

    step_query = query_blk * jnp.exp(logdec_blk)
    identity_blk = jnp.eye(block_len, dtype=jnp.float32)
    erase_write = paired(erase_blk, write_blk)
    erase_key = paired(erase_blk, key_blk)
    read_write = (
        paired(step_query, write_blk)
        + identity_blk * jnp.sum(query_blk * write_blk, axis=-1)[:, :, None]
    )
    read_key = (
        paired(step_query, key_blk)
        + identity_blk * jnp.sum(query_blk * key_blk, axis=-1)[:, :, None]
    )
    inverse = identity_blk + erase_write
    power = erase_write
    for level in range(block_len.bit_length() - 2):
        power = exact_mul("hts,hsu->htu", power, power)
        inverse = inverse + exact_mul("hts,hsu->htu", inverse, power)
    erase_hat = erase_blk * jnp.exp(log_before)
    query_hat = query_blk * jnp.exp(log_gain)
    total_gain = log_gain[:, -1:, :]
    to_end = jnp.exp(total_gain - log_gain)
    write_end = write_blk * to_end
    key_end = key_blk * to_end
    pulled = exact_mul("hts,hsv->htv", inverse, exact_mul("hts,hsv->htv", erase_key, value_blk))
    local_out = exact_mul("hts,hsv->htv", read_write, pulled) + exact_mul(
        "hts,hsv->htv", read_key, value_blk
    )
    psi_block = exact_mul("hsv,hsc->hvc", pulled, write_end) + exact_mul(
        "hsv,hsc->hvc", value_blk, key_end
    )
    erase_solved = exact_mul("hts,hsc->htc", inverse, erase_hat)
    query_full = query_hat + exact_mul("hts,hsc->htc", read_write, erase_solved)
    identity_key = jnp.eye(head_size, dtype=jnp.float32)
    phi_block = jnp.exp(total_gain[:, 0, :])[:, :, None] * identity_key + exact_mul(
        "hsc,hsd->hcd", erase_solved, write_end
    )
    local_out = local_out + exact_mul("htc,hvc->htv", query_full, psi_sofar)
    carried_query = exact_mul("htc,hdc->htd", query_full, phi_sofar)
    phi_next = exact_mul("hcd,hde->hce", phi_sofar, phi_block)
    psi_next = exact_mul("hvd,hde->hve", psi_sofar, phi_block) + psi_block
    return ((phi_next, psi_next), (local_out, carried_query))


def body(
    tokens,
    input_norm_gain,
    query_matrix,
    key_matrix,
    value_matrix,
    convolution_value_matrix,
    convolution_gate_matrix,
    decay_offset_channel,
    decay_first_matrix,
    decay_second_matrix,
    learning_rate_offset,
    learning_rate_first_matrix,
    learning_rate_second_matrix,
    forgetting_rate_factor,
    state_retention_share,
    per_head_norm_gain,
    convolution_filter_taps,
    convolution_channel_gain,
    attention_output_matrix,
    convolution_output_matrix,
):
    tok_rows = tokens.shape[0]
    heads_dev = forgetting_rate_factor.shape[1]
    head_size = query_matrix.shape[1] // heads_dev
    widened = tokens.astype(jnp.float32)
    normed = (
        widened
        * lax.rsqrt(jnp.mean(widened * widened, axis=-1, keepdims=True) + RMS_EPSILON)
        * input_norm_gain
    ).astype(jnp.bfloat16)
    pieces = in_one_piece(
        (query_matrix, key_matrix, value_matrix, convolution_value_matrix, convolution_gate_matrix),
        SP,
        0,
        1,
    )
    query_proj, key_proj, value_proj, conv_value, conv_gate = tuple(
        (jnp.dot(normed, piece, preferred_element_type=jnp.float32) for piece in pieces)
    )
    decay_mid = jnp.tanh(
        jnp.dot(normed, decay_first_matrix, preferred_element_type=jnp.float32)
    ).astype(jnp.bfloat16)
    rate_mid = jnp.dot(
        normed, learning_rate_first_matrix, preferred_element_type=jnp.float32
    ).astype(jnp.bfloat16)
    logarithm_learning_rate = (
        -jax.nn.softplus(
            -(
                decay_offset_channel
                + jnp.dot(decay_mid, decay_second_matrix, preferred_element_type=jnp.float32)
            )
        )
        - 0.5
    )
    learn_rate = jax.nn.sigmoid(
        learning_rate_offset
        + jnp.dot(rate_mid, learning_rate_second_matrix, preferred_element_type=jnp.float32)
    )
    reshaped_tensor = (tok_rows, heads_dev, head_size)
    log_decay = (
        -jnp.exp(logarithm_learning_rate).reshape(reshaped_tensor)
        * forgetting_rate_factor[:, :, None]
        + jnp.log(state_retention_share)[:, :, None]
    )
    key_heads = key_proj.reshape(reshaped_tensor)
    unit_key = key_heads * lax.rsqrt(
        jnp.sum(key_heads * key_heads, axis=-1, keepdims=True) + UNIT_EPSILON
    )
    erase = -unit_key
    write = unit_key * learn_rate.reshape(reshaped_tensor)
    block_len = math.gcd(tok_rows, 128)
    block_count = tok_rows // block_len
    inputs = tuple(
        (
            split_blocks(item, block_count, block_len)
            for item in (
                query_proj.reshape(reshaped_tensor),
                log_decay,
                key_heads,
                value_proj.reshape(reshaped_tensor),
                erase,
                write,
            )
        )
    )
    identity_key = jnp.broadcast_to(
        jnp.eye(head_size, dtype=jnp.float32), (heads_dev, head_size, head_size)
    )
    device_pair, block_outs = lax.scan(
        block_update, (identity_key, jnp.zeros_like(identity_key)), inputs
    )
    local_out, carried_query = block_outs
    phi_device, psi_device = device_pair
    prefix = prefix_by_axis(
        (phi_device, psi_device), SP, chain_pair, (identity_key, jnp.zeros_like(identity_key))
    )
    state_in = prefix[1]
    state_out = local_out + exact_mul("bhtd,hvd->bhtv", carried_query, state_in)
    state_rows = state_out.transpose(0, 2, 1, 3).reshape(reshaped_tensor)
    centred = state_rows - jnp.mean(state_rows, axis=-1, keepdims=True)
    normal_state = centred * lax.rsqrt(
        jnp.mean(centred * centred, axis=-1, keepdims=True) + GROUP_EPSILON
    )
    state_mixed = (
        (normal_state * per_head_norm_gain.reshape(heads_dev, head_size))
        .reshape(tok_rows, heads_dev * head_size)
        .astype(jnp.bfloat16)
    )
    gated = (conv_value * jax.nn.sigmoid(conv_gate)).astype(jnp.bfloat16)
    span = convolution_filter_taps.shape[0]
    rim = from_behind(gated[tok_rows - (span - 1) :], SP, 1)
    padded = jnp.concatenate([rim, gated], axis=0)
    filtered = jnp.zeros(gated.shape, jnp.float32)
    for offset in range(span):
        filtered = filtered + convolution_filter_taps[offset] * padded[offset : offset + tok_rows]
    total_sum, total_square = lax.psum(
        (jnp.sum(filtered, axis=-1), jnp.sum(filtered * filtered, axis=-1)), "tp"
    )
    row_mean = total_sum / CONV_CH
    deviation = filtered - row_mean[:, None]
    variance = total_square / CONV_CH - row_mean * row_mean
    conv_mixed = jax.nn.silu(
        deviation * lax.rsqrt(variance + LAYER_EPSILON)[:, None] * convolution_channel_gain
    ).astype(jnp.bfloat16)
    contract_dims = (((1,), (1,)), ((), ()))
    pieces = sent_together((attention_output_matrix, convolution_output_matrix), SP, 0, 1)
    partial_out = lax.dot_general(
        state_mixed, pieces[0], contract_dims, preferred_element_type=jnp.float32
    ) + lax.dot_general(conv_mixed, pieces[1], contract_dims, preferred_element_type=jnp.float32)
    return (
        total_of_pieces(partial_out.astype(jnp.bfloat16), "tp")
        .astype(jnp.float32)
        .astype(jnp.bfloat16)
    )


def solution(mesh):
    finer = Mesh(mesh.devices.reshape(16, 4, mesh.shape["tp"]), ("sp_0", "sp_1", "tp"))
    return jax.shard_map(
        body,
        mesh=finer,
        in_specs=(
            P(SP, None),
            P(),
            P(SP, "tp"),
            P(SP, "tp"),
            P(SP, "tp"),
            P(SP, "tp"),
            P(SP, "tp"),
            P("tp"),
            P(),
            P(None, "tp"),
            P("tp"),
            P(),
            P(None, "tp"),
            P(SP, "tp"),
            P(SP, "tp"),
            P("tp"),
            P(None, "tp"),
            P("tp"),
            P(SP, "tp"),
            P(SP, "tp"),
        ),
        out_specs=P(SP, None),
        check_vma=False,
    )
```

profile of v0, /device:TPU:1, one launch (start us, length us, event | category | flops | bytes accessed | tf_op | source)
XLA Modules:
  0.0 448.9 jit_solution(8406004709652950613)
XLA Ops:
  12.4 1.6 fusion.73
  14.1 1.9 fusion.86
  17.1 135.3 %all-gather.7.cloned.1.call-done = bf16[2048,896]{1,0:T(8,128)(2,1)} async-done(((bf16[32,896]{1,0:T(8,128)(2,1)}), bf16[2048,896]{1,0:T(8,128)(2,1)}) %all-gather.7.cloned.1.call-update) | async-done | bytes 3670032 | tf_op jit(solution)/shard_map/all_gather | solution.py:23
  152.4 1.6 fusion.97
  154.1 1.6 fusion.99
  155.8 1.6 bitcast_reduce_fusion
  157.7 92.0 %while.17 = (s32[]{:T(128)}, f32[2,64,64]{1,2,0:T(8,128)S(1)}, f32[2,64,64]{1,2,0:T(8,128)S(1)}, f32[2,2,128,64]{2,3,0,1:T(8,128)}, f32[2,2,128,64]{2,3,0,1:T(8,...) while((s32[]{:T(128)}, f32[2,64,64]{1,2,0:T(8,128)S(1)}, ...), condition=%wide.region_6.7_spmd.clone, body=%wide.region_2.6_spmd.clone.sunk | while | flops 959192576 | bytes 13395232 | solution.py:265
  159.3 7.9 %fusion.448 = f32[2,128,1,128]{3,2,1,0:T(1,128)S(1)} fusion(f32[2,128,64,1]{2,3,1,0:T(1,128)S(1)} %copy.180, f32[2,128,64]{1,2,0:T(8,128)S(1)} %bitcast.450, f32[2,128,64]{1,2,0:T(8,128)S(1)} %copy.178, f32[2,128,64]{2,1,0:T(8,128)S(1)} %copy.179, pred[128,128]{1,0:T(8,128)(4,1)S(1)} %iota_compare_fusion.5), kind=kOutput, calls=%fused_computation.clone.1 | convolution fusion | flops 31457280 | bytes 409600 | tf_op jit(solution)/shard_map/while/body/eval_jaxpr/htc,htsc,hsc->hts/dot_general | solution.py:131
  167.2 8.3 %fusion.446 = f32[2,128,1,128]{3,2,1,0:T(1,128)S(1)} fusion(f32[2,128,64,1]{2,3,1,0:T(1,128)S(1)} %copy.180, f32[2,128,64]{1,2,0:T(8,128)S(1)} %bitcast.436, f32[2,128,64]{1,2,0:T(8,128)S(1)} %copy.178, f32[2,128,64]{2,1,0:T(8,128)S(1)} %copy.179, pred[128,128]{1,0:T(8,128)(4,1)S(1)} %iota_compare_fusion.5), kind=kOutput, calls=%fused_computation.4.clone.1 | convolution fusion | flops 31457280 | bytes 409600 | tf_op jit(solution)/shard_map/while/body/eval_jaxpr/htc,htsc,hsc->hts/dot_general | solution.py:131
  175.5 8.1 %fusion.441 = f32[2,128,1,128]{3,2,1,0:T(1,128)S(1)} fusion(f32[2,128,64,1]{2,3,1,0:T(1,128)S(1)} %copy.176, f32[2,128,64]{1,2,0:T(8,128)S(1)} %bitcast.451, f32[2,128,64]{1,2,0:T(8,128)S(1)} %copy.178, f32[2,128,64]{2,1,0:T(8,128)S(1)} %copy.179, pred[128,128]{1,0:T(8,128)(4,1)S(1)} %iota_compare_fusion.5), kind=kOutput, calls=%fused_computation.2.clone.1 | convolution fusion | flops 31457280 | bytes 409600 | tf_op jit(solution)/shard_map/while/body/eval_jaxpr/htc,htsc,hsc->hts/dot_general | solution.py:131
  183.7 7.9 %fusion.431 = f32[2,128,1,128]{3,2,1,0:T(1,128)S(1)} fusion(f32[2,128,64,1]{2,3,1,0:T(1,128)S(1)} %copy.176, f32[2,128,64]{1,2,0:T(8,128)S(1)} %bitcast.437, f32[2,128,64]{1,2,0:T(8,128)S(1)} %copy.178, f32[2,128,64]{2,1,0:T(8,128)S(1)} %copy.179, pred[128,128]{1,0:T(8,128)(4,1)S(1)} %iota_compare_fusion.5), kind=kOutput, calls=%fused_computation.6.clone.1 | convolution fusion | flops 31457280 | bytes 409600 | tf_op jit(solution)/shard_map/while/body/eval_jaxpr/htc,htsc,hsc->hts/dot_general | solution.py:131
  201.5 7.9 %fusion.448 = f32[2,128,1,128]{3,2,1,0:T(1,128)S(1)} fusion(f32[2,128,64,1]{2,3,1,0:T(1,128)S(1)} %copy.180, f32[2,128,64]{1,2,0:T(8,128)S(1)} %bitcast.450, f32[2,128,64]{1,2,0:T(8,128)S(1)} %copy.178, f32[2,128,64]{2,1,0:T(8,128)S(1)} %copy.179, pred[128,128]{1,0:T(8,128)(4,1)S(1)} %iota_compare_fusion.5), kind=kOutput, calls=%fused_computation.clone.1 | convolution fusion | flops 31457280 | bytes 409600 | tf_op jit(solution)/shard_map/while/body/eval_jaxpr/htc,htsc,hsc->hts/dot_general | solution.py:131
  209.4 8.1 %fusion.446 = f32[2,128,1,128]{3,2,1,0:T(1,128)S(1)} fusion(f32[2,128,64,1]{2,3,1,0:T(1,128)S(1)} %copy.180, f32[2,128,64]{1,2,0:T(8,128)S(1)} %bitcast.436, f32[2,128,64]{1,2,0:T(8,128)S(1)} %copy.178, f32[2,128,64]{2,1,0:T(8,128)S(1)} %copy.179, pred[128,128]{1,0:T(8,128)(4,1)S(1)} %iota_compare_fusion.5), kind=kOutput, calls=%fused_computation.4.clone.1 | convolution fusion | flops 31457280 | bytes 409600 | tf_op jit(solution)/shard_map/while/body/eval_jaxpr/htc,htsc,hsc->hts/dot_general | solution.py:131
  217.5 8.3 %fusion.441 = f32[2,128,1,128]{3,2,1,0:T(1,128)S(1)} fusion(f32[2,128,64,1]{2,3,1,0:T(1,128)S(1)} %copy.176, f32[2,128,64]{1,2,0:T(8,128)S(1)} %bitcast.451, f32[2,128,64]{1,2,0:T(8,128)S(1)} %copy.178, f32[2,128,64]{2,1,0:T(8,128)S(1)} %copy.179, pred[128,128]{1,0:T(8,128)(4,1)S(1)} %iota_compare_fusion.5), kind=kOutput, calls=%fused_computation.2.clone.1 | convolution fusion | flops 31457280 | bytes 409600 | tf_op jit(solution)/shard_map/while/body/eval_jaxpr/htc,htsc,hsc->hts/dot_general | solution.py:131
  225.9 7.9 %fusion.431 = f32[2,128,1,128]{3,2,1,0:T(1,128)S(1)} fusion(f32[2,128,64,1]{2,3,1,0:T(1,128)S(1)} %copy.176, f32[2,128,64]{1,2,0:T(8,128)S(1)} %bitcast.437, f32[2,128,64]{1,2,0:T(8,128)S(1)} %copy.178, f32[2,128,64]{2,1,0:T(8,128)S(1)} %copy.179, pred[128,128]{1,0:T(8,128)(4,1)S(1)} %iota_compare_fusion.5), kind=kOutput, calls=%fused_computation.6.clone.1 | convolution fusion | flops 31457280 | bytes 409600 | tf_op jit(solution)/shard_map/while/body/eval_jaxpr/htc,htsc,hsc->hts/dot_general | solution.py:131
  250.0 9.4 %all-gather = f32[1024,64]{0,1:T(8,128)S(1)} all-gather(f32[256,64]{0,1:T(8,128)S(1)} %pad_maximum_fusion.2), channel_id=2, replica_groups=mesh['sp_0'=16,'sp_1'=4,'tp'=8] {'sp_1'}, dimensions={0}, use_global_device_ids=true | all-gather | bytes 327680 | tf_op jit(solution)/shard_map/all_gather | solution.py:41
  263.3 8.1 %all-to-all-start = ((bf16[64,32,384]{2,1,0:T(8,128)(2,1)}), bf16[64,32,384]{2,1,0:T(8,128)(2,1)S(1)}, u32[]{:S(2)}, u32[]{:S(2)}) async-start(bf16[64,32,384]{2,1,0:T(8,128)(2,1)} %broadcast_in_dim.44), calls=%async_computation | async-start | bytes 3145728 | tf_op jit(solution)/shard_map/all_to_all | solution.py:73
  271.6 1.7 fusion.93
  273.4 1.7 fusion.80
  275.1 2.9 collective-permute-start
  280.1 26.6 %all-reduce = (f32[256]{0:T(256)S(1)}, f32[256]{0:T(256)S(1)}) all-reduce(f32[256]{0:T(256)S(1)} %get-tuple-element.141, f32[256]{0:T(256)S(1)} %get-tuple-element.140), channel_id=1, replica_groups=mesh['sp_0'=16,'sp_1'=4,'tp'=8] {'tp'}, use_global_device_ids=true, to_apply=%region_12.13 | all-reduce | flops 512 | bytes 4096 | tf_op jit(solution)/shard_map/psum | solution.py:292
  306.7 62.8 %all-gather.9.cloned.1.call-done = f32[4096,64]{1,0:T(8,128)} async-done(((f32[256,64]{1,0:T(8,128)}), f32[4096,64]{1,0:T(8,128)}) %all-gather.9.cloned.1.call-update) | async-done | bytes 1048592 | tf_op jit(solution)/shard_map/all_gather | solution.py:41
  377.3 58.4 %all-gather.11.cloned.1.call-done = bf16[2048,2048]{1,0:T(8,128)(2,1)} async-done(((bf16[256,2048]{1,0:T(8,128)(2,1)}), bf16[2048,2048]{1,0:T(8,128)(2,1)}) %all-gather.11.cloned.1.call-update) | async-done | bytes 8388624 | tf_op jit(solution)/shard_map/all_gather | solution.py:97
  435.7 6.4 %reduce_sum.90 = bf16[256,2048]{1,0:T(8,128)(2,1)} reduce(bf16[8,256,2048]{2,1,0:T(8,128)(2,1)} %bitcast.455, bf16[]{:T(256)} %constant.97.clone.1), dimensions={0}, to_apply=%region_13.14 | reduce | flops 3670016 | bytes 9437186 | tf_op jit(solution)/shard_map/reduce_sum | solution.py:97
  (232 shorter events, 39.2 us)
Async XLA Ops:
  6.5 7.5 %copy-start = (bf16[2048,128]{1,0:T(8,128)(2,1)S(1)}, bf16[2048,128]{1,0:T(8,128)(2,1)}, u32[]{:S(2)}) copy-start(bf16[2048,128]{1,0:T(8,128)(2,1)} %param.33) | copy-start | bytes 1572868
  6.5 145.8 %all-gather.7.cloned.1.call-start = ((), (), s32[]{:S(2)}) async-start(), calls=%async_computation.1 | async-start | bytes 3727360 | tf_op jit(solution)/shard_map/all_gather | solution.py:23
  10.8 358.7 %all-gather.9.cloned.1.call-start = ((), (), s32[]{:S(2)}) async-start(), calls=%async_computation.2 | async-start | bytes 2228224 | tf_op jit(solution)/shard_map/all_gather | solution.py:41
  12.3 3.8 copy-start.2
  12.4 3.8 copy-start.23
  12.4 3.8 copy-start.24
  12.4 3.8 copy-start.25
  12.4 3.8 copy-start.26
  194.2 4.1 copy-start.14
  194.5 4.4 copy-start.11
  236.4 4.1 copy-start.14
  236.7 4.4 copy-start.11
  250.0 12.0 %copy-start.19 = (bf16[32,256]{1,0:T(8,128)(2,1)S(1)}, bf16[32,256]{1,0:T(8,128)(2,1)}, u32[]{:S(2)}) copy-start(bf16[32,256]{1,0:T(8,128)(2,1)} %param.41) | copy-start | bytes 49156
  250.0 12.0 %copy-start.20 = (bf16[32,128]{1,0:T(8,128)(2,1)S(1)}, bf16[32,128]{1,0:T(8,128)(2,1)}, u32[]{:S(2)}) copy-start(bf16[32,128]{1,0:T(8,128)(2,1)} %param.40) | copy-start | bytes 24580
  260.1 3.3 copy-start.3
  260.5 2.9 copy-start.5
  260.9 2.5 copy-start.7
  262.0 9.6 %copy-start.18 = (f32[31,256]{1,0:T(8,128)S(1)}, f32[31,256]{1,0:T(8,128)}, u32[]{:S(2)}) copy-start(f32[31,256]{1,0:T(8,128)} %param.38) | copy-start | bytes 95236
  263.3 112.0 %all-to-all-start = ((bf16[64,32,384]{2,1,0:T(8,128)(2,1)}), bf16[64,32,384]{2,1,0:T(8,128)(2,1)S(1)}, u32[]{:S(2)}, u32[]{:S(2)}) async-start(bf16[64,32,384]{2,1,0:T(8,128)(2,1)} %broadcast_in_dim.44), calls=%async_computation | async-start | bytes 3145728 | tf_op jit(solution)/shard_map/all_to_all | solution.py:73
  271.5 164.3 %all-gather.11.cloned.1.call-start = ((), (), s32[]{:S(2)}) async-start(), calls=%async_computation.3 | async-start | bytes 9437184 | tf_op jit(solution)/shard_map/all_gather | solution.py:97
  275.1 3.8 collective-permute-start
  369.5 2.6 copy-start.1
  372.2 2.5 copy-start.13
  372.2 2.5 copy-start.16
  (12 other events, 18.4 us)
Sparse Core Ops, SparseCore 0:
  10.9 141.4 all-gather.6
  262.1 107.3 all-gather.8
  377.4 58.2 all-gather.10
where the time goes:
time: 453 us; the launch traced here: 449 us
  waiting for transfers between devices  257 us (57%)
  matrix products  98.3 us (22%)
  blocking collectives  35.9 us (8%)
  between operations  14.2 us (3%)
  local copies, waits for them, and re-layouts  12.3 us (3%)
  starting transfers between devices  11.1 us (2%)
  other arithmetic  10.7 us (2%)
  loops' own time  9.06 us (2%)
    all_gather x1, waiting for transfers between devices, in_one_piece(): out = lax.all_gather(both, axis, axis=dim, tiled=True)  135 us
    dot_general x8, matrix products, paired(): jnp.einsum('htc,htsc,hsc->hts', left, pair_decay, right, precision=HIGHEST)  64.7 us
    all_gather x1, waiting for transfers between devices, collected_together(): both, at, found = (lax.all_gather(jnp.concatenate(lines), axis), 0, {})  62.8 us
    all_gather x1, waiting for transfers between devices, total_of_pieces(): return lax.all_gather(x, axis).astype(jnp.float32).sum(0)  58.4 us
    psum x1, blocking collectives, body(): lax.psum((jnp.sum(filtered, axis=-1), jnp.sum(filtered * filtered, axis=-...  26.6 us
    dot_general x78, matrix products, exact_mul(): return jnp.einsum(form, left, right, precision=HIGHEST)  20.8 us
    all_gather x1, blocking collectives, collected_together(): both, at, found = (lax.all_gather(jnp.concatenate(lines), axis), 0, {})  9.37 us
    another operation x1, loops' own time, body(): lax.scan(block_update, (identity_key, jnp.zeros_like(identity_key)), inputs)  9.06 us
  transfers between devices with their start and end apart: 5, of which 4 were waited for; matrix products, arithmetic and copies ran while one was open for 4% of the time, Pallas kernels for 0%

commit v1 on v0

v1 whole, which is shorter than its diff:
```python
import jax
import jax.numpy as jnp
from jax import lax
from jax.experimental import pallas as pl
from jax.experimental.pallas import tpu as pltpu
from jax.sharding import Mesh
from jax.sharding import PartitionSpec as P

BF = jnp.bfloat16
F32 = jnp.float32
NN = (((1,), (0,)), ((), ()))
NT = (((1,), (1,)), ((), ()))
TN = (((0,), (0,)), ((), ()))

SP = ("za", "zb", "zc", "y")
Z = ("za", "zb", "zc")
TP = ("x", "c")
FAR = ("za", "zb")
NEAR = ("zc", "y")
RMS_EPSILON = 1e-06
GROUP_EPSILON = 0.00064
LAYER_EPSILON = 1e-05
UNIT_EPSILON = 1e-06

TOK = 256
HALO = 32
RB = 32
DIM = 2048
STATS = 16


def dot1(a, b, dims=NN):
    return lax.dot_general(a.astype(BF), b.astype(BF), dims, preferred_element_type=F32)


def two(a):
    hi = a.astype(BF)
    return hi, (a - hi.astype(F32)).astype(BF)


def dot3(a, b, dims=NN):
    ah, al = two(a)
    bh, bl = two(b)
    one = lambda l, r: lax.dot_general(l, r, dims, preferred_element_type=F32)
    return one(ah, bh) + (one(ah, bl) + one(al, bh))


def three(a):
    hi = a.astype(BF)
    rest = a - hi.astype(F32)
    mid = rest.astype(BF)
    return hi, mid, (rest - mid.astype(F32)).astype(BF)


def lanes(shape):
    return lax.broadcasted_iota(jnp.int32, shape, len(shape) - 1)


def rows(shape):
    return lax.broadcasted_iota(jnp.int32, shape, 0)


def by_head(pair, shape):
    return jnp.where(lanes(shape) < 64, pair[:, 0:1], pair[:, 1:2])


def head_sum(a):
    first = lanes(a.shape) < 64
    s0 = jnp.sum(jnp.where(first, a, 0.0), axis=1, keepdims=True)
    s1 = jnp.sum(jnp.where(first, 0.0, a), axis=1, keepdims=True)
    return jnp.where(first, s0, s1)


def rms_rows(x, gain):
    x = x.astype(F32)
    scale = lax.rsqrt(jnp.mean(x * x, axis=-1, keepdims=True) + RMS_EPSILON)
    return (x * scale * gain).astype(BF)


def norm_kernel(tok, gain, df, ds, do, lf, ls, lo, fr, sr, normed, rates):
    x = rms_rows(tok[...], gain[...])
    normed[...] = x
    mid = jnp.tanh(dot1(x, df[...])).astype(BF)
    pre = do[...] + dot1(mid, ds[...])
    rate = 0.6065306597126334 / (1.0 + jnp.exp(-pre))
    step = by_head(jnp.log(sr[...]), rate.shape) - rate * by_head(fr[...], rate.shape)
    rates[0] = step
    low = (rows((TOK, TOK)) >= lanes((TOK, TOK))).astype(BF)
    h, m, l = three(step)
    rates[1] = dot1(low, h) + (dot1(low, m) + dot1(low, l))
    mid2 = dot1(x, lf[...]).astype(BF)
    pre2 = lo[...] + dot1(mid2, ls[...])
    rates[2] = 1.0 / (1.0 + jnp.exp(-pre2))


def in_row_order(w, ws):
    for y in range(4):
        for z in range(16):
            ws[z, y] = w[y, z]


def state_kernel(x, w, rates, parts, trans, ws, ew, ek, qw, qk):
    in_row_order(w, ws)
    proj = dot1(x[...], ws[...].reshape(DIM, 384))
    q, k, v = proj[:, :128], proj[:, 128:256], proj[:, 256:]
    g = rates[1]
    before = g - rates[0]
    unit = k * lax.rsqrt(head_sum(k * k) + UNIT_EPSILON)
    er = -unit
    wr = unit * rates[2]
    first32 = lanes((RB, 128)) < 64
    for i in range(TOK // RB):
        lo, hi = i * RB, (i + 1) * RB
        width = 128 if hi <= 128 else 256
        ref = g[lo + RB // 2 - 1 : lo + RB // 2]
        le = er[lo:hi] * jnp.exp(before[lo:hi] - ref)
        lq = q[lo:hi] * jnp.exp(g[lo:hi] - ref)
        left = jnp.concatenate(
            [
                jnp.where(first32, le, 0.0),
                jnp.where(first32, 0.0, le),
                jnp.where(first32, lq, 0.0),
                jnp.where(first32, 0.0, lq),
            ],
            axis=0,
        ).astype(BF)
        dec = jnp.exp(jnp.minimum(ref - g[:width], 60.0))
        pw = dot1(left, wr[:width] * dec, NT)
        pk = dot1(left, k[:width] * dec, NT)
        t = rows((RB, width)) + lo
        s = lanes((RB, width))
        strict, incl = t > s, t >= s
        for h in range(2):
            a, b = h * RB, (h + 1) * RB
            c, d = (2 + h) * RB, (3 + h) * RB
            ew[h, lo:hi, :width] = jnp.where(strict, pw[a:b], 0.0).astype(BF)
            ek[h, lo:hi, :width] = jnp.where(strict, pk[a:b], 0.0)
            qw[h, lo:hi, :width] = jnp.where(incl, pw[c:d], 0.0)
            qk[h, lo:hi, :width] = jnp.where(incl, pk[c:d], 0.0)
            if width < TOK:
                zero = jnp.zeros((RB, TOK - width), F32)
                ew[h, lo:hi, width:] = zero.astype(BF)
                ek[h, lo:hi, width:] = zero
                qw[h, lo:hi, width:] = zero
                qk[h, lo:hi, width:] = zero
    t = rows((TOK, TOK))
    s = lanes((TOK, TOK))

    def same(n):
        return (t // n) == (s // n)

    invs = []
    base = [jnp.where(same(8), ew[h], jnp.zeros((), BF)) for h in range(2)]
    sq = [dot1(n8, n8) for n8 in base]
    eye = (t == s).astype(F32)
    cube = [dot1(n8, n2) for n8, n2 in zip(base, sq)]
    four = [dot1(n2, n2) for n2 in sq]
    part = [eye + n8.astype(F32) + n2 + n3 for n8, n2, n3 in zip(base, sq, cube)]
    invs = [p + dot1(p, n4) for p, n4 in zip(part, four)]
    for n in (8, 16, 32, 64):
        off = same(2 * n) & ~same(n)
        xs = [
            dot1(jnp.where(off, ew[h], jnp.zeros((), BF)), invs[h])
            for h in range(2)
        ]
        invs = [inv + dot1(inv, xx) for inv, xx in zip(invs, xs)]
    first = lanes((TOK, 128)) < 64
    ehat = er * jnp.exp(before)
    qhat = q * jnp.exp(g)
    last = g[TOK - 1 : TOK]
    toend = jnp.exp(last - g)
    wend = wr * toend
    kend = k * toend
    vsw = pltpu.roll(v, 64, axis=1)
    ys, zs = [], []
    for h in range(2):
        own = first if h == 0 else ~first
        r = jnp.where(own, ehat, dot3(ek[h], vsw))
        inv = invs[h]
        x1 = dot3(inv[:128, :128], r[:128])
        r2 = r[128:] + dot3(ew[h, 128:, :128].astype(F32), x1)
        x2 = dot3(inv[128:, 128:], r2)
        xx = jnp.concatenate([x1, x2], axis=0)
        ys.append(dot3(qw[h], xx) + jnp.where(own, qhat, dot3(qk[h], vsw)))
        zz = dot3(xx, wend, TN)
        zs.append(zz if h == 0 else jnp.concatenate([zz[64:], zz[:64]], axis=0))
    parts[0] = jnp.where(first, ys[0], ys[1])
    parts[1] = pltpu.roll(jnp.where(first, ys[1], ys[0]), 64, axis=1)
    vk = dot3(v, kend, TN)
    half = lanes((64, 128)) < 64
    diag = (lanes((64, 128)) % 64) == rows((64, 128))
    dpart = jnp.where(half, zs[0][:64], zs[1][:64]) + jnp.where(diag, jnp.exp(last) - 1.0, 0.0)
    ppart = jnp.where(half, zs[0][64:] + vk[:64], zs[1][64:] + vk[64:])
    trans[...] = jnp.concatenate([dpart, ppart], axis=0).astype(BF)


def two_blocks(a):
    half = lanes((64, 128)) < 64
    return jnp.concatenate([jnp.where(half, a, 0.0), jnp.where(half, 0.0, a)], axis=0)


def chain(earlier, later):
    d, p = earlier
    turn = two_blocks(later[0])
    d, p = d + later[0] + dot3(d, turn), p + later[1] + dot3(p, turn)
    return jnp.minimum(d, 3e38), jnp.minimum(p, 3e38)


def fold(pieces):
    while len(pieces) > 1:
        pieces = [chain(pieces[k], pieces[k + 1]) for k in range(0, len(pieces), 2)]
    return pieces[0]


def unpacked(ref):
    return [(ref[k, :64].astype(F32), ref[k, 64:].astype(F32)) for k in range(8)]


def passed(place, pieces):
    keep = [place[0] > k for k in range(8)]
    return [(jnp.where(on, d, 0.0), jnp.where(on, p, 0.0)) for on, (d, p) in zip(keep, pieces)]


def prefix_kernel(place, pieces, total, prefix):
    each = unpacked(pieces)
    d, p = fold(each)
    total[:64] = d.astype(BF)
    total[64:] = p.astype(BF)
    d, p = fold(passed(place, each))
    prefix[:64] = d
    prefix[64:] = p


def finish_kernel(place, pieces, before, parts, gain, dev, pay):
    inside = fold(passed(place, unpacked(pieces)))
    state = chain(inside, (before[:64], before[64:]))[1]
    y = parts[1] + dot3(parts[0], two_blocks(state), NT)
    c = y - head_sum(y) * (1.0 / 64.0)
    n = c * lax.rsqrt(head_sum(c * c) * (1.0 / 64.0) + GROUP_EPSILON)
    mixed = (n * gain[...]).astype(BF)
    pay[: TOK + STATS] = dev[...]
    pay[TOK + STATS :, :128] = mixed[:128]
    pay[TOK + STATS :, 128:] = mixed[128:]


def from_neighbours(place, pieces, ws):
    for k, piece in enumerate(pieces):
        y = lax.rem(place[0] + 4 - k, 4)
        for z in range(16):
            ws[z, y] = piece[z]


def conv_kernel(place, x, halo, gain, w0, w1, w2, w3, taps, cgain, out, ws, gs):
    from_neighbours(place, (w0, w1, w2, w3), ws)
    wide = ws[...].reshape(DIM, 512)
    ph = dot1(rms_rows(halo[...], gain[...]), wide)
    pm = dot1(x[...], wide)

    def gate(p):
        return (p[:, :256] / (1.0 + jnp.exp(-p[:, 256:]))).astype(BF).astype(F32)

    gs[:HALO] = gate(ph)
    gs[HALO:] = gate(pm)
    acc = jnp.zeros((TOK, 256), F32)
    for j in range(31):
        acc = acc + taps[j : j + 1] * gs[pl.ds(2 + j, TOK), :]
    mean = jnp.mean(acc, axis=1, keepdims=True)
    dev = acc - mean
    sq = jnp.sum(dev * dev, axis=1, keepdims=True)
    out[:TOK] = dev.astype(BF)
    parts = [p.astype(F32) for p in (*three(mean), *three(sq))]
    col = lanes((TOK, 128))
    grid = jnp.zeros((TOK, 128), F32)
    for k, p in enumerate(parts):
        grid = jnp.where(col == k, p, grid)
    low = jnp.transpose(grid)[:STATS]
    r = rows((STATS, 256))
    for k, p in enumerate(three(cgain[...])):
        low = jnp.where(r == 6 + k, p.astype(F32), low)
    out[TOK:] = low.astype(BF)


def final_kernel(place, pay, w0, w1, w2, w3, out, shifts):
    low = pay[:, TOK : TOK + STATS].astype(F32).reshape(8 * STATS, 256)
    cols = jnp.transpose(low)

    def stat(g, k):
        c = g * STATS + k
        return cols[:, c : c + 1] + cols[:, c + 1 : c + 2] + cols[:, c + 2 : c + 3]

    means = [stat(g, 0) for g in range(8)]
    mean = sum(means) * 0.125
    var = sum(stat(g, 3) for g in range(8))
    var = (var + 256.0 * sum((m - mean) * (m - mean) for m in means)) * (1.0 / 2048.0)
    inv = lax.rsqrt(var + LAYER_EPSILON)
    for g in range(8):
        shifts[g] = jnp.broadcast_to((means[g] - mean) * inv, (TOK, 128))
    total = jnp.zeros((TOK, 256), F32)
    for k, piece in enumerate((w0, w1, w2, w3)):
        y = lax.rem(place[0] + 4 - k, 4)
        for half in range(2):
            g = 2 * y + half
            w = piece[8 * half : 8 * half + 8].reshape(256, 384)
            head = pay[g, TOK : TOK + STATS].astype(F32)
            gain = head[6:7] + head[7:8] + head[8:9]
            shift = shifts[g]
            u = pay[g, :TOK].astype(F32) * inv + jnp.concatenate([shift, shift], axis=1)
            u = u * gain
            u = u / (1.0 + jnp.exp(-u))
            total = total + dot1(u, w[:, 128:], NT)
            m = pay[g, TOK + STATS :]
            m = jnp.concatenate([m[:, :128], m[:, 128:]], axis=0)
            total = total + dot1(m, w[:, :128], NT)
    out[...] = total.astype(BF)


def place_kernel(place, own, other, out, sems):
    c = place[0]
    copies = []
    for x in range(4):
        for k, (src, core) in enumerate(((own, c), (other, 1 - c))):
            at = pl.multiple_of((2 * x + core) * 256, 256)
            copies.append(
                pltpu.make_async_copy(src.at[x], out.at[:, pl.ds(at, 256)], sems.at[2 * x + k])
            )
    for copy in copies:
        copy.start()
    for copy in copies:
        copy.wait()


VM = pl.BlockSpec(memory_space=pltpu.VMEM)
SM = pl.BlockSpec(memory_space=pltpu.SMEM)


def call(kernel, outs, args, scratch=(), smem=0):
    return pl.pallas_call(
        kernel,
        out_shape=[jax.ShapeDtypeStruct(s, d) for s, d in outs],
        in_specs=[SM] * smem + [VM] * (len(args) - smem),
        out_specs=[VM] * len(outs),
        scratch_shapes=list(scratch),
        compiler_params=pltpu.CompilerParams(vmem_limit_bytes=24 * 1024 * 1024),
    )(*args)


def everyone(x, axis):
    size = lax.axis_size(axis)
    copies = jnp.broadcast_to(x, (size, *x.shape))
    return lax.all_to_all(copies, axis, split_axis=0, concat_axis=0, tiled=True)


def placed(axis):
    return lax.axis_index(axis).reshape(1).astype(jnp.int32)


def neighbours(x):
    pieces = [x]
    for k in (1, 2, 3):
        pieces.append(lax.ppermute(x, "y", [(i, (i + k) % 4) for i in range(4)]))
    return pieces


def layer(
    tokens,
    input_norm_gain,
    query_matrix,
    key_matrix,
    value_matrix,
    convolution_value_matrix,
    convolution_gate_matrix,
    decay_offset_channel,
    decay_first_matrix,
    decay_second_matrix,
    learning_rate_offset,
    learning_rate_first_matrix,
    learning_rate_second_matrix,
    forgetting_rate_factor,
    state_retention_share,
    per_head_norm_gain,
    convolution_filter_taps,
    convolution_channel_gain,
    attention_output_matrix,
    convolution_output_matrix,
):
    row = lambda a: a.reshape(1, -1)
    gain = row(input_norm_gain)
    w_state = jnp.concatenate([query_matrix, key_matrix, value_matrix], axis=1)
    w_out = jnp.concatenate([attention_output_matrix, convolution_output_matrix], axis=1)
    w_state = everyone(everyone(w_state, Z), "y")
    halo = lax.ppermute(tokens[TOK - HALO :], SP, [(i, i + 1) for i in range(63)])
    moves = []
    for a in range(8):
        for b in range(8):
            for j in range(8):
                target = ((j % 2) * 8 + b) * 4 + j // 2
                moves.append(((8 * a + b) * 8 + j, target * 8 + a))
    w_out = lax.ppermute(w_out, (*SP, *TP), moves)
    rest = jnp.concatenate([convolution_value_matrix, convolution_gate_matrix, w_out], axis=1)
    rest = lax.all_gather(rest, Z)
    w_conv = neighbours(rest[..., :512])
    w_out = neighbours(rest[..., 512:])

    normed, rates = call(
        norm_kernel,
        [((TOK, DIM), BF), ((3, TOK, 128), F32)],
        (
            tokens,
            gain,
            decay_first_matrix,
            decay_second_matrix,
            row(decay_offset_channel),
            learning_rate_first_matrix,
            learning_rate_second_matrix,
            row(learning_rate_offset),
            forgetting_rate_factor,
            state_retention_share,
        ),
    )
    square = pltpu.VMEM((2, TOK, TOK), F32)
    parts, trans = call(
        state_kernel,
        [((2, TOK, 128), F32), ((128, 128), BF)],
        (normed, w_state, rates),
        [pltpu.VMEM((16, 4, 32, 384), BF), pltpu.VMEM((2, TOK, TOK), BF), square, square, square],
    )

    total, before = call(
        prefix_kernel,
        [((128, 128), BF), ((128, 128), F32)],
        (placed(NEAR), everyone(trans, NEAR)),
        smem=1,
    )
    y = placed("y")
    (dev,) = call(
        conv_kernel,
        [((TOK + STATS, 256), BF)],
        (y, normed, halo, gain, *w_conv, convolution_filter_taps, row(convolution_channel_gain)),
        [pltpu.VMEM((16, 4, 32, 512), BF), pltpu.VMEM((TOK + HALO, 256), F32)],
        smem=1,
    )
    (pay,) = call(
        finish_kernel,
        [((TOK + STATS + 128, 256), BF)],
        (placed(FAR), everyone(total, FAR), before, parts, row(per_head_norm_gain), dev),
        smem=1,
    )
    (out,) = call(
        final_kernel,
        [((TOK, 256), BF)],
        (y, everyone(pay, TP), *w_out),
        [pltpu.VMEM((8, TOK, 128), F32)],
        smem=1,
    )
    own = everyone(out, "x")
    other = lax.ppermute(own, "c", [(0, 1), (1, 0)])
    hbm = pl.BlockSpec(memory_space=pl.ANY)
    return pl.pallas_call(
        place_kernel,
        out_shape=jax.ShapeDtypeStruct((TOK, DIM), BF),
        in_specs=[SM, VM, VM],
        out_specs=hbm,
        scratch_shapes=[pltpu.SemaphoreType.DMA((8,))],
        name="place",
    )(placed("c"), own, other)


def solution(mesh):
    finer = Mesh(mesh.devices.reshape(4, 2, 2, 4, 4, 2), (*SP, *TP))
    return jax.shard_map(
        layer,
        mesh=finer,
        in_specs=(
            P(SP, None),
            P(),
            P(SP, TP),
            P(SP, TP),
            P(SP, TP),
            P(SP, TP),
            P(SP, TP),
            P(TP),
            P(),
            P(None, TP),
            P(TP),
            P(),
            P(None, TP),
            P(SP, TP),
            P(SP, TP),
            P(TP),
            P(None, TP),
            P(TP),
            P(SP, TP),
            P(SP, TP),
        ),
        out_specs=P(SP, None),
        check_vma=False,
    )
```

time: 453 us -> 230 us (0.51)
  waiting for transfers between devices: 257 us -> 33.4 us
  matrix products: 98.3 us -> 0 us
  starting transfers between devices: 11.1 us -> 81.8 us
  blocking collectives: 35.9 us -> 81.7 us
  Pallas kernels: 0 us -> 18.7 us
  between operations: 14.2 us -> 0.53 us
  other arithmetic: 10.7 us -> 0.75 us
  loops' own time: 9.06 us -> 0 us
    all_gather x3 -> x0, waiting for transfers between devices: 257 us -> none  [the longest x1 135 us: in_one_piece(): out = lax.all_gather(both, axis, axis=dim, tiled=True)]
    dot_general x95 -> x0, matrix products: 98.3 us -> none  [the longest x8 64.7 us: paired(): jnp.einsum('htc,htsc,hsc->hts', left, pair_decay, right, precision=HIGHEST)]
    all_to_all x0 -> x2, blocking collectives: none -> 44.9 us  [everyone(): return lax.all_to_all(copies, axis, split_axis=0, concat_axis=0, tiled=True)]
    ppermute x1 -> x9, starting transfers between devices: 2.92 us -> 41.8 us  [the longest x6 22.9 us: neighbours(): pieces.append(lax.ppermute(x, 'y', [(i, (i + k) % 4) for i in range(4)]))]
    all_to_all x1 -> x4, starting transfers between devices: 8.13 us -> 40 us  [everyone(): return lax.all_to_all(copies, axis, split_axis=0, concat_axis=0, tiled=True)]
    all_gather x1, blocking collectives: 9.37 us -> 36.7 us  [layer(): rest = lax.all_gather(rest, Z)]
    psum x1 -> x0, blocking collectives: 26.6 us -> none  [body(): lax.psum((jnp.sum(filtered, axis=-1), jnp.sum(filtered * filtered, axis=-...]
    ppermute x1 -> x9, waiting for transfers between devices: 0.65 us -> 24.7 us  [the longest x6 16.5 us: neighbours(): pieces.append(lax.ppermute(x, 'y', [(i, (i + k) % 4) for i in range(4)]))]
  transfers between devices with their start and end apart: 5 -> 13, of which waited for: 4 -> 9; matrix products, arithmetic and copies ran while one was open for 4% -> 1% of each run, Pallas kernels for 0% -> 2%
where the time goes in v1:
time: 230 us; the launch traced here: 228 us
  starting transfers between devices  81.8 us (36%)
  blocking collectives  81.7 us (36%)
  waiting for transfers between devices  33.4 us (15%)
  Pallas kernels  18.7 us (8%)
  local copies, waits for them, and re-layouts  11.4 us (5%)
    all_to_all x2, blocking collectives, everyone(): return lax.all_to_all(copies, axis, split_axis=0, concat_axis=0, tiled=True)  44.9 us
    all_to_all x4, starting transfers between devices, everyone(): return lax.all_to_all(copies, axis, split_axis=0, concat_axis=0, tiled=True)  40 us
    all_gather x1, blocking collectives, layer(): rest = lax.all_gather(rest, Z)  36.7 us
    ppermute x6, starting transfers between devices, neighbours(): pieces.append(lax.ppermute(x, 'y', [(i, (i + k) % 4) for i in range(4)]))  22.9 us
    pallas_call x6, Pallas kernels, call(): pl.pallas_call(kernel, out_shape=[jax.ShapeDtypeStruct(s, d) for s, d in...  16.5 us
    ppermute x6, waiting for transfers between devices, neighbours(): pieces.append(lax.ppermute(x, 'y', [(i, (i + k) % 4) for i in range(4)]))  16.5 us
    ppermute x1, starting transfers between devices, layer(): w_out = lax.ppermute(w_out, (*SP, *TP), moves)  12.3 us
    all_to_all x4, waiting for transfers between devices, everyone(): return lax.all_to_all(copies, axis, split_axis=0, concat_axis=0, tiled=True)  8.68 us
  transfers between devices with their start and end apart: 13, of which 9 were waited for; matrix products, arithmetic and copies ran while one was open for 1% of the time, Pallas kernels for 2%

profile of v1, /device:TPU:1, one launch (start us, length us, event | category | flops | bytes accessed | tf_op | source)
XLA Modules:
  0.0 228.2 jit_solution(1278096931272962531)
XLA Ops:
  0.8 33.6 %all_to_all.30 = bf16[16,32,384]{2,1,0:T(8,128)(2,1)S(1)} all-to-all(bf16[16,32,384]{2,1,0:T(8,128)(2,1)S(1)} %broadcast_in_dim.18), channel_id=1, replica_groups=mesh['za'=4,'zb'=2,'zc'=2,'y'=4,'x'=4,'c'=2] {'za','zb','zc'}, dimensions={0} | all-to-all | bytes 786432 | tf_op jit(solution)/shard_map/all_to_all | solution.py:350
  35.8 4.3 %all-to-all-start.1 = ((bf16[4,16,32,384]{3,2,1,0:T(8,128)(2,1)}), bf16[4,16,32,384]{3,2,1,0:T(8,128)(2,1)S(1)}, u32[]{:S(2)}, u32[]{:S(2)}) async-start(bf16[4,16,32,384]{3,2,1,0:T(8,128)(2,1)} %broadcast_in_dim.19), calls=%async_computation.1 | async-start | bytes 3145728 | tf_op jit(solution)/shard_map/all_to_all | solution.py:350
  45.1 8.7 %all-to-all-done.1.w = bf16[4,16,32,384]{3,2,1,0:T(8,128)(2,1)S(1)} async-done(((bf16[4,16,32,384]{3,2,1,0:T(8,128)(2,1)}), bf16[4,16,32,384]{3,2,1,0:T(8,128)(2,1)S(1)}, u32[]{:S(2)}, u32[]{:S(2)}) %all-to-all-start.1) | async-done | bytes 1572896 | tf_op jit(solution)/shard_map/all_to_all | solution.py:350
  54.8 5.6 %shard_map.191 = (f32[2,256,128]{2,1,0:T(8,128)S(1)}, bf16[128,128]{1,0:T(8,128)(2,1)S(1)}) custom-call(bf16[256,2048]{1,0:T(8,128)(2,1)S(1)} %get-tuple-element.11.x, bf16[4,16,32,384]{3,2,1,0:T(8,128)(2,1)S(1)} %all-to-all-done.1.w, f32[3,256,128]{2,1,0:T(8,128)S(1)} %copy-done.4), custom_call_target="tpu_custom_call" | custom-call | tf_op jit(solution)/shard_map/pallas_call | solution.py:337
  61.1 11.1 %all-to-all-start.2 = ((bf16[8,128,128]{2,1,0:T(8,128)(2,1)}), bf16[8,128,128]{2,1,0:T(8,128)(2,1)S(1)}, u32[]{:S(2)}, u32[]{:S(2)}) async-start(bf16[8,128,128]{2,1,0:T(8,128)(2,1)} %broadcast_in_dim.20), calls=%async_computation.2 | async-start | bytes 524288 | tf_op jit(solution)/shard_map/all_to_all | solution.py:350
  72.2 12.3 %collective-permute-start.1 = (bf16[32,384]{1,0:T(8,128)(2,1)S(1)}, bf16[32,384]{1,0:T(8,128)(2,1)S(1)}, u32[]{:S(2)}, u32[]{:S(2)}) collective-permute-start(bf16[32,384]{1,0:T(8,128)(2,1)S(1)} %pad_maximum_fusion.2), channel_id=1, source_target_pairs={{0,0},{1,256},{2,8},{3,264},{4,16},{5,272},{6,24},{7,280},{8,32},{... | collective-permute-start | bytes 73736 | tf_op jit(solution)/shard_map/ppermute | solution.py:398
  87.6 10.7 %all-to-all-start.3 = ((bf16[8,128,128]{2,1,0:T(8,128)(2,1)}), bf16[8,128,128]{2,1,0:T(8,128)(2,1)S(1)}, u32[]{:S(2)}, u32[]{:S(2)}) async-start(bf16[8,128,128]{2,1,0:T(8,128)(2,1)} %broadcast_in_dim.21), calls=%async_computation.3 | async-start | bytes 524288 | tf_op jit(solution)/shard_map/all_to_all | solution.py:350
  98.3 36.7 %all-gather = bf16[512,896]{1,0:T(8,128)(2,1)S(1)} all-gather(bf16[32,896]{1,0:T(8,128)(2,1)S(1)} %pad_maximum_fusion), channel_id=2, replica_groups=mesh['za'=4,'zb'=2,'zc'=2,'y'=4,'x'=4,'c'=2] {'za','zb','zc'}, dimensions={0}, use_global_device_ids=true | all-gather | bytes 974848 | tf_op jit(solution)/shard_map/all_gather | solution.py:400
  135.1 3.3 %collective-permute-start.2 = (bf16[16,32,512]{2,1,0:T(8,128)(2,1)S(1)}, bf16[16,32,512]{2,1,0:T(8,128)(2,1)S(1)}, u32[]{:S(2)}, u32[]{:S(2)}) collective-permute-start(bf16[16,32,512]{2,1,0:T(8,128)(2,1)S(1)} %slice.12.w0), channel_id=1, source_target_pairs={{0,8},{8,16},{16,24},{24,0},{1,9},{9,17},{17,25},{25,1},{2,10},{10... | collective-permute-start | bytes 1572872 | tf_op jit(solution)/shard_map/ppermute | solution.py:360
  138.4 6.0 %collective-permute-start.3 = (bf16[16,32,512]{2,1,0:T(8,128)(2,1)S(1)}, bf16[16,32,512]{2,1,0:T(8,128)(2,1)S(1)}, u32[]{:S(2)}, u32[]{:S(2)}) collective-permute-start(bf16[16,32,512]{2,1,0:T(8,128)(2,1)S(1)} %slice.12.w0), channel_id=1, source_target_pairs={{0,16},{8,24},{16,0},{24,8},{1,17},{9,25},{17,1},{25,9},{2,18},{10... | collective-permute-start | bytes 1572872 | tf_op jit(solution)/shard_map/ppermute | solution.py:360
  144.5 3.3 %collective-permute-start.4 = (bf16[16,32,512]{2,1,0:T(8,128)(2,1)S(1)}, bf16[16,32,512]{2,1,0:T(8,128)(2,1)}, u32[]{:S(2)}, u32[]{:S(2)}) collective-permute-start(bf16[16,32,512]{2,1,0:T(8,128)(2,1)S(1)} %slice.12.w0), channel_id=1, source_target_pairs={{0,24},{8,0},{16,8},{24,16},{1,25},{9,1},{17,9},{25,17},{2,26},{10... | collective-permute-start | bytes 1572872 | tf_op jit(solution)/shard_map/ppermute | solution.py:360
  148.7 2.0 collective-permute-start
  150.7 5.7 %collective-permute-done.halo = bf16[32,2048]{1,0:T(8,128)(2,1)S(1)} collective-permute-done((bf16[32,2048]{1,0:T(8,128)(2,1)S(1)}, bf16[32,2048]{1,0:T(8,128)(2,1)S(1)}, u32[]{:S(2)}, u32[]{:S(2)}) %collective-permute-start) | collective-permute-done | bytes 131104 | tf_op jit(solution)/shard_map/ppermute | solution.py:391
  158.6 3.9 %shard_map.193.dev = bf16[272,256]{1,0:T(8,128)(2,1)S(1)} custom-call(s32[1]{0:T(128)} %bitcast.1.place, bf16[256,2048]{1,0:T(8,128)(2,1)S(1)} %get-tuple-element.11.x, bf16[32,2048]{1,0:T(8,128)(2,1)S(1)} %collective-permute-done.halo, f32[1,2048]{1,0:T(1,128)S(1)} %bitcast.11, bf16[16,32,512]{2,1,0:T(8,128)(2,1)S(1)} %slice.12.w0, ...), custom_call_target="tpu_custom_call" | custom-call | tf_op jit(solution)/shard_map/pallas_call | solution.py:337
  165.1 13.9 %all-to-all-start.4 = ((bf16[8,400,256]{2,1,0:T(8,128)(2,1)}), bf16[8,400,256]{2,1,0:T(8,128)(2,1)S(1)}, u32[]{:S(2)}, u32[]{:S(2)}) async-start(bf16[8,400,256]{2,1,0:T(8,128)(2,1)} %broadcast_in_dim.22), calls=%async_computation.4 | async-start | bytes 3276800 | tf_op jit(solution)/shard_map/all_to_all | solution.py:350
  180.1 3.7 %collective-permute-start.5 = (bf16[16,32,384]{2,1,0:T(8,128)(2,1)S(1)}, bf16[16,32,384]{2,1,0:T(8,128)(2,1)S(1)}, u32[]{:S(2)}, u32[]{:S(2)}) collective-permute-start(bf16[16,32,384]{2,1,0:T(8,128)(2,1)S(1)} %slice.13.w0), channel_id=1, source_target_pairs={{0,8},{8,16},{16,24},{24,0},{1,9},{9,17},{17,25},{25,1},{2,10},{10... | collective-permute-start | bytes 1179656 | tf_op jit(solution)/shard_map/ppermute | solution.py:360
  183.7 3.8 %collective-permute-start.6 = (bf16[16,32,384]{2,1,0:T(8,128)(2,1)S(1)}, bf16[16,32,384]{2,1,0:T(8,128)(2,1)S(1)}, u32[]{:S(2)}, u32[]{:S(2)}) collective-permute-start(bf16[16,32,384]{2,1,0:T(8,128)(2,1)S(1)} %slice.13.w0), channel_id=1, source_target_pairs={{0,16},{8,24},{16,0},{24,8},{1,17},{9,25},{17,1},{25,9},{2,18},{10... | collective-permute-start | bytes 1179656 | tf_op jit(solution)/shard_map/ppermute | solution.py:360
  187.6 2.7 %collective-permute-start.7 = (bf16[16,32,384]{2,1,0:T(8,128)(2,1)S(1)}, bf16[16,32,384]{2,1,0:T(8,128)(2,1)S(1)}, u32[]{:S(2)}, u32[]{:S(2)}) collective-permute-start(bf16[16,32,384]{2,1,0:T(8,128)(2,1)S(1)} %slice.13.w0), channel_id=1, source_target_pairs={{0,24},{8,0},{16,8},{24,16},{1,25},{9,1},{17,9},{25,17},{2,26},{10... | collective-permute-start | bytes 1179656 | tf_op jit(solution)/shard_map/ppermute | solution.py:360
  190.3 3.5 %collective-permute-done.5.w1 = bf16[16,32,384]{2,1,0:T(8,128)(2,1)S(1)} collective-permute-done((bf16[16,32,384]{2,1,0:T(8,128)(2,1)S(1)}, bf16[16,32,384]{2,1,0:T(8,128)(2,1)S(1)}, u32[]{:S(2)}, u32[]{:S(2)}) %collective-permute-start.5) | collective-permute-done | bytes 393248 | tf_op jit(solution)/shard_map/ppermute | solution.py:360
  193.8 9.2 %collective-permute-done.6.w2 = bf16[16,32,384]{2,1,0:T(8,128)(2,1)S(1)} collective-permute-done((bf16[16,32,384]{2,1,0:T(8,128)(2,1)S(1)}, bf16[16,32,384]{2,1,0:T(8,128)(2,1)S(1)}, u32[]{:S(2)}, u32[]{:S(2)}) %collective-permute-start.6) | collective-permute-done | bytes 393248 | tf_op jit(solution)/shard_map/ppermute | solution.py:360
  204.7 2.9 %shard_map.195 = bf16[256,256]{1,0:T(8,128)(2,1)S(1)} custom-call(s32[1]{0:T(128)} %bitcast.1.place, bf16[8,400,256]{2,1,0:T(8,128)(2,1)S(1)} %all-to-all-done.4.pay, bf16[16,32,384]{2,1,0:T(8,128)(2,1)S(1)} %slice.13.w0, bf16[16,32,384]{2,1,0:T(8,128)(2,1)S(1)} %collective-permute-done.5.w1, bf16[16,32,384]{2,1,0:T(8,128)(2,1)S(1)} %collective-permute-done.6.w2, ...), custom_call_target="tpu_custom_call" | custom-call | tf_op jit(solution)/shard_map/pallas_call | solution.py:337
  207.6 11.3 %all_to_all.31.own = bf16[4,256,256]{2,1,0:T(8,128)(2,1)S(1)} all-to-all(bf16[4,256,256]{2,1,0:T(8,128)(2,1)S(1)} %broadcast_in_dim.23), channel_id=1, replica_groups=mesh['za'=4,'zb'=2,'zc'=2,'y'=4,'x'=4,'c'=2] {'x'}, dimensions={0} | all-to-all | bytes 1048576 | tf_op jit(solution)/shard_map/all_to_all | solution.py:350
  218.9 4.6 %collective-permute-start.8 = (bf16[4,256,256]{2,1,0:T(8,128)(2,1)S(1)}, bf16[4,256,256]{2,1,0:T(8,128)(2,1)S(1)}, u32[]{:S(2)}, u32[]{:S(2)}) collective-permute-start(bf16[4,256,256]{2,1,0:T(8,128)(2,1)S(1)} %all_to_all.31.own), channel_id=1, source_target_pairs={{0,1},{1,0},{2,3},{3,2},{4,5},{5,4},{6,7},{7,6},{8,9},{9,8},{10,11... | collective-permute-start | bytes 1572872 | tf_op jit(solution)/shard_map/ppermute | solution.py:456
  225.8 2.2 place.1
  (70 shorter events, 22.4 us)
Async XLA Ops:
  35.8 4.7 %copy-start.6 = (bf16[128,128]{1,0:T(8,128)(2,1)S(1)}, bf16[128,128]{1,0:T(8,128)(2,1)}, u32[]{:S(2)}) copy-start(bf16[128,128]{1,0:T(8,128)(2,1)} %ls.1) | copy-start | bytes 98308
  35.8 4.7 %copy-start.8 = (f32[2048]{0:T(1024)S(1)}, f32[2048]{0:T(1024)}, u32[]{:S(2)}) copy-start(f32[2048]{0:T(1024)} %param.21) | copy-start | bytes 24580
  35.8 4.7 %copy-start.10 = (f32[128]{0:T(128)S(1)}, f32[128]{0:T(128)}, u32[]{:S(2)}) copy-start(f32[128]{0:T(128)} %param.27) | copy-start | bytes 1540
  35.8 17.9 %all-to-all-start.1 = ((bf16[4,16,32,384]{3,2,1,0:T(8,128)(2,1)}), bf16[4,16,32,384]{3,2,1,0:T(8,128)(2,1)S(1)}, u32[]{:S(2)}, u32[]{:S(2)}) async-start(bf16[4,16,32,384]{3,2,1,0:T(8,128)(2,1)} %broadcast_in_dim.19), calls=%async_computation.1 | async-start | bytes 3145728 | tf_op jit(solution)/shard_map/all_to_all | solution.py:350
  54.7 17.5 %copy-start.16 = (bf16[32,256]{1,0:T(8,128)(2,1)S(1)}, bf16[32,256]{1,0:T(8,128)(2,1)}, u32[]{:S(2)}) copy-start(bf16[32,256]{1,0:T(8,128)(2,1)} %param.39) | copy-start | bytes 49156
  54.7 17.5 %copy-start.19 = (bf16[32,128]{1,0:T(8,128)(2,1)S(1)}, bf16[32,128]{1,0:T(8,128)(2,1)}, u32[]{:S(2)}) copy-start(bf16[32,128]{1,0:T(8,128)(2,1)} %param.38) | copy-start | bytes 24580
  54.7 30.7 %copy-start.17 = (bf16[32,256]{1,0:T(8,128)(2,1)S(1)}, bf16[32,256]{1,0:T(8,128)(2,1)}, u32[]{:S(2)}) copy-start(bf16[32,256]{1,0:T(8,128)(2,1)} %param.26) | copy-start | bytes 49156
  54.8 30.7 %copy-start.18 = (bf16[32,256]{1,0:T(8,128)(2,1)S(1)}, bf16[32,256]{1,0:T(8,128)(2,1)}, u32[]{:S(2)}) copy-start(bf16[32,256]{1,0:T(8,128)(2,1)} %param.25) | copy-start | bytes 49156
  61.1 24.4 %all-to-all-start.2 = ((bf16[8,128,128]{2,1,0:T(8,128)(2,1)}), bf16[8,128,128]{2,1,0:T(8,128)(2,1)S(1)}, u32[]{:S(2)}, u32[]{:S(2)}) async-start(bf16[8,128,128]{2,1,0:T(8,128)(2,1)} %broadcast_in_dim.20), calls=%async_computation.2 | async-start | bytes 524288 | tf_op jit(solution)/shard_map/all_to_all | solution.py:350
  72.2 13.3 %collective-permute-start.1 = (bf16[32,384]{1,0:T(8,128)(2,1)S(1)}, bf16[32,384]{1,0:T(8,128)(2,1)S(1)}, u32[]{:S(2)}, u32[]{:S(2)}) collective-permute-start(bf16[32,384]{1,0:T(8,128)(2,1)S(1)} %pad_maximum_fusion.2), channel_id=1, source_target_pairs={{0,0},{1,256},{2,8},{3,264},{4,16},{5,272},{6,24},{7,280},{8,32},{... | collective-permute-start | bytes 73736 | tf_op jit(solution)/shard_map/ppermute | solution.py:398
  85.5 73.1 %copy-start.7 = (f32[31,256]{1,0:T(8,128)S(1)}, f32[31,256]{1,0:T(8,128)}, u32[]{:S(2)}) copy-start(f32[31,256]{1,0:T(8,128)} %taps.1) | copy-start | bytes 95236
  85.5 73.1 %copy-start.9 = (f32[256]{0:T(256)S(1)}, f32[256]{0:T(256)}, u32[]{:S(2)}) copy-start(f32[256]{0:T(256)} %param.37) | copy-start | bytes 3076
  87.6 75.0 %all-to-all-start.3 = ((bf16[8,128,128]{2,1,0:T(8,128)(2,1)}), bf16[8,128,128]{2,1,0:T(8,128)(2,1)S(1)}, u32[]{:S(2)}, u32[]{:S(2)}) async-start(bf16[8,128,128]{2,1,0:T(8,128)(2,1)} %broadcast_in_dim.21), calls=%async_computation.3 | async-start | bytes 524288 | tf_op jit(solution)/shard_map/all_to_all | solution.py:350
  135.0 12.7 %copy-start.13 = (bf16[512,896]{1,0:T(8,128)(2,1)}, bf16[512,896]{1,0:T(8,128)(2,1)S(1)}, u32[]{:S(2)}) copy-start(bf16[512,896]{1,0:T(8,128)(2,1)S(1)} %all-gather) | copy-start | bytes 2752516
  135.1 21.4 %collective-permute-start.2 = (bf16[16,32,512]{2,1,0:T(8,128)(2,1)S(1)}, bf16[16,32,512]{2,1,0:T(8,128)(2,1)S(1)}, u32[]{:S(2)}, u32[]{:S(2)}) collective-permute-start(bf16[16,32,512]{2,1,0:T(8,128)(2,1)S(1)} %slice.12.w0), channel_id=1, source_target_pairs={{0,8},{8,16},{16,24},{24,0},{1,9},{9,17},{17,25},{25,1},{2,10},{10... | collective-permute-start | bytes 1572872 | tf_op jit(solution)/shard_map/ppermute | solution.py:360
  138.4 18.6 %collective-permute-start.3 = (bf16[16,32,512]{2,1,0:T(8,128)(2,1)S(1)}, bf16[16,32,512]{2,1,0:T(8,128)(2,1)S(1)}, u32[]{:S(2)}, u32[]{:S(2)}) collective-permute-start(bf16[16,32,512]{2,1,0:T(8,128)(2,1)S(1)} %slice.12.w0), channel_id=1, source_target_pairs={{0,16},{8,24},{16,0},{24,8},{1,17},{9,25},{17,1},{25,9},{2,18},{10... | collective-permute-start | bytes 1572872 | tf_op jit(solution)/shard_map/ppermute | solution.py:360
  144.5 14.1 %collective-permute-start.4 = (bf16[16,32,512]{2,1,0:T(8,128)(2,1)S(1)}, bf16[16,32,512]{2,1,0:T(8,128)(2,1)}, u32[]{:S(2)}, u32[]{:S(2)}) collective-permute-start(bf16[16,32,512]{2,1,0:T(8,128)(2,1)S(1)} %slice.12.w0), channel_id=1, source_target_pairs={{0,24},{8,0},{16,8},{24,16},{1,25},{9,1},{17,9},{25,17},{2,26},{10... | collective-permute-start | bytes 1572872 | tf_op jit(solution)/shard_map/ppermute | solution.py:360
  148.7 7.8 %collective-permute-start = (bf16[32,2048]{1,0:T(8,128)(2,1)S(1)}, bf16[32,2048]{1,0:T(8,128)(2,1)S(1)}, u32[]{:S(2)}, u32[]{:S(2)}) collective-permute-start(bf16[32,2048]{1,0:T(8,128)(2,1)S(1)} %slice.9), channel_id=1, source_target_pairs={{0,8},{8,16},{16,24},{24,32},{32,40},{40,48},{48,56},{56,64},{64,7... | collective-permute-start | bytes 393224 | tf_op jit(solution)/shard_map/ppermute | solution.py:391
  165.1 39.6 %all-to-all-start.4 = ((bf16[8,400,256]{2,1,0:T(8,128)(2,1)}), bf16[8,400,256]{2,1,0:T(8,128)(2,1)S(1)}, u32[]{:S(2)}, u32[]{:S(2)}) async-start(bf16[8,400,256]{2,1,0:T(8,128)(2,1)} %broadcast_in_dim.22), calls=%async_computation.4 | async-start | bytes 3276800 | tf_op jit(solution)/shard_map/all_to_all | solution.py:350
  180.1 13.8 %collective-permute-start.5 = (bf16[16,32,384]{2,1,0:T(8,128)(2,1)S(1)}, bf16[16,32,384]{2,1,0:T(8,128)(2,1)S(1)}, u32[]{:S(2)}, u32[]{:S(2)}) collective-permute-start(bf16[16,32,384]{2,1,0:T(8,128)(2,1)S(1)} %slice.13.w0), channel_id=1, source_target_pairs={{0,8},{8,16},{16,24},{24,0},{1,9},{9,17},{17,25},{25,1},{2,10},{10... | collective-permute-start | bytes 1179656 | tf_op jit(solution)/shard_map/ppermute | solution.py:360
  183.7 19.4 %collective-permute-start.6 = (bf16[16,32,384]{2,1,0:T(8,128)(2,1)S(1)}, bf16[16,32,384]{2,1,0:T(8,128)(2,1)S(1)}, u32[]{:S(2)}, u32[]{:S(2)}) collective-permute-start(bf16[16,32,384]{2,1,0:T(8,128)(2,1)S(1)} %slice.13.w0), channel_id=1, source_target_pairs={{0,16},{8,24},{16,0},{24,8},{1,17},{9,25},{17,1},{25,9},{2,18},{10... | collective-permute-start | bytes 1179656 | tf_op jit(solution)/shard_map/ppermute | solution.py:360
  187.6 17.1 %collective-permute-start.7 = (bf16[16,32,384]{2,1,0:T(8,128)(2,1)S(1)}, bf16[16,32,384]{2,1,0:T(8,128)(2,1)S(1)}, u32[]{:S(2)}, u32[]{:S(2)}) collective-permute-start(bf16[16,32,384]{2,1,0:T(8,128)(2,1)S(1)} %slice.13.w0), channel_id=1, source_target_pairs={{0,24},{8,0},{16,8},{24,16},{1,25},{9,1},{17,9},{25,17},{2,26},{10... | collective-permute-start | bytes 1179656 | tf_op jit(solution)/shard_map/ppermute | solution.py:360
  218.9 6.1 %copy-start.14 = (bf16[4,256,256]{2,1,0:T(8,128)(2,1)}, bf16[4,256,256]{2,1,0:T(8,128)(2,1)S(1)}, u32[]{:S(2)}) copy-start(bf16[4,256,256]{2,1,0:T(8,128)(2,1)S(1)} %all_to_all.31.own) | copy-start | bytes 1572868
  218.9 6.1 %collective-permute-start.8 = (bf16[4,256,256]{2,1,0:T(8,128)(2,1)S(1)}, bf16[4,256,256]{2,1,0:T(8,128)(2,1)S(1)}, u32[]{:S(2)}, u32[]{:S(2)}) collective-permute-start(bf16[4,256,256]{2,1,0:T(8,128)(2,1)S(1)} %all_to_all.31.own), channel_id=1, source_target_pairs={{0,1},{1,0},{2,3},{3,2},{4,5},{5,4},{6,7},{7,6},{8,9},{9,8},{10,11... | collective-permute-start | bytes 1572872 | tf_op jit(solution)/shard_map/ppermute | solution.py:456
  (11 other events, 31.7 us)

commit v2 on v1

--- a/solution.py
+++ b/solution.py
@@ -191,7 +191,9 @@
     diag = (lanes((64, 128)) % 64) == rows((64, 128))
     dpart = jnp.where(half, zs[0][:64], zs[1][:64]) + jnp.where(diag, jnp.exp(last) - 1.0, 0.0)
     ppart = jnp.where(half, zs[0][64:] + vk[:64], zs[1][64:] + vk[64:])
-    trans[...] = jnp.concatenate([dpart, ppart], axis=0).astype(BF)
+    mine = jnp.concatenate([dpart, ppart], axis=0).astype(BF)
+    for k in range(8):
+        trans[k] = mine
 
 
 def two_blocks(a):
@@ -224,8 +226,10 @@
 def prefix_kernel(place, pieces, total, prefix):
     each = unpacked(pieces)
     d, p = fold(each)
-    total[:64] = d.astype(BF)
-    total[64:] = p.astype(BF)
+    d, p = d.astype(BF), p.astype(BF)
+    for k in range(8):
+        total[k, :64] = d
+        total[k, 64:] = p
     d, p = fold(passed(place, each))
     prefix[:64] = d
     prefix[64:] = p
@@ -238,9 +242,11 @@
     c = y - head_sum(y) * (1.0 / 64.0)
     n = c * lax.rsqrt(head_sum(c * c) * (1.0 / 64.0) + GROUP_EPSILON)
     mixed = (n * gain[...]).astype(BF)
-    pay[: TOK + STATS] = dev[...]
-    pay[TOK + STATS :, :128] = mixed[:128]
-    pay[TOK + STATS :, 128:] = mixed[128:]
+    rows_ = dev[...]
+    for k in range(4):
+        pay[k, : TOK + STATS] = rows_
+        pay[k, TOK + STATS :, :128] = mixed[:128]
+        pay[k, TOK + STATS :, 128:] = mixed[128:]
 
 
 def from_neighbours(place, pieces, ws):
@@ -280,8 +286,10 @@
     out[TOK:] = low.astype(BF)
 
 
-def final_kernel(place, pay, w0, w1, w2, w3, out, shifts):
-    low = pay[:, TOK : TOK + STATS].astype(F32).reshape(8 * STATS, 256)
+def final_kernel(place, core, own, other, w0, w1, w2, w3, out, shifts):
+    low = jnp.concatenate(
+        [p[:, TOK : TOK + STATS].astype(F32).reshape(4 * STATS, 256) for p in (own, other)], axis=0
+    )
     cols = jnp.transpose(low)
 
     def stat(g, k):
@@ -297,21 +305,23 @@
         shifts[g] = jnp.broadcast_to((means[g] - mean) * inv, (TOK, 128))
     total = jnp.zeros((TOK, 256), F32)
     for k, piece in enumerate((w0, w1, w2, w3)):
-        y = lax.rem(place[0] + 4 - k, 4)
-        for half in range(2):
-            g = 2 * y + half
-            w = piece[8 * half : 8 * half + 8].reshape(256, 384)
-            head = pay[g, TOK : TOK + STATS].astype(F32)
+        x = lax.rem(place[0] + 4 - k, 4)
+        for n, pay in enumerate((own, other)):
+            half = core[0] if n == 0 else 1 - core[0]
+            w = piece[pl.ds(half * 8, 8)].reshape(256, 384)
+            head = pay[x, TOK : TOK + STATS].astype(F32)
             gain = head[6:7] + head[7:8] + head[8:9]
-            shift = shifts[g]
-            u = pay[g, :TOK].astype(F32) * inv + jnp.concatenate([shift, shift], axis=1)
+            shift = shifts[4 * n + x]
+            u = pay[x, :TOK].astype(F32) * inv + jnp.concatenate([shift, shift], axis=1)
             u = u * gain
             u = u / (1.0 + jnp.exp(-u))
             total = total + dot1(u, w[:, 128:], NT)
-            m = pay[g, TOK + STATS :]
+            m = pay[x, TOK + STATS :]
             m = jnp.concatenate([m[:, :128], m[:, 128:]], axis=0)
             total = total + dot1(m, w[:, :128], NT)
-    out[...] = total.astype(BF)
+    total = total.astype(BF)
+    for k in range(4):
+        out[k] = total
 
 
 def place_kernel(place, own, other, out, sems):
@@ -348,6 +358,14 @@
     size = lax.axis_size(axis)
     copies = jnp.broadcast_to(x, (size, *x.shape))
     return lax.all_to_all(copies, axis, split_axis=0, concat_axis=0, tiled=True)
+
+
+def exchange(copies, axis):
+    return lax.all_to_all(copies, axis, split_axis=0, concat_axis=0, tiled=True)
+
+
+def other_core(x):
+    return lax.ppermute(x, "c", [(0, 1), (1, 0)])
 
 
 def placed(axis):
@@ -420,15 +438,15 @@
     square = pltpu.VMEM((2, TOK, TOK), F32)
     parts, trans = call(
         state_kernel,
-        [((2, TOK, 128), F32), ((128, 128), BF)],
+        [((2, TOK, 128), F32), ((8, 128, 128), BF)],
         (normed, w_state, rates),
         [pltpu.VMEM((16, 4, 32, 384), BF), pltpu.VMEM((2, TOK, TOK), BF), square, square, square],
     )
 
     total, before = call(
         prefix_kernel,
-        [((128, 128), BF), ((128, 128), F32)],
-        (placed(NEAR), everyone(trans, NEAR)),
+        [((8, 128, 128), BF), ((128, 128), F32)],
+        (placed(NEAR), exchange(trans, NEAR)),
         smem=1,
     )
     y = placed("y")
@@ -441,19 +459,20 @@
     )
     (pay,) = call(
         finish_kernel,
-        [((TOK + STATS + 128, 256), BF)],
-        (placed(FAR), everyone(total, FAR), before, parts, row(per_head_norm_gain), dev),
+        [((4, TOK + STATS + 128, 256), BF)],
+        (placed(FAR), exchange(total, FAR), before, parts, row(per_head_norm_gain), dev),
         smem=1,
     )
+    pay = exchange(pay, "x")
     (out,) = call(
         final_kernel,
-        [((TOK, 256), BF)],
-        (y, everyone(pay, TP), *w_out),
+        [((4, TOK, 256), BF)],
+        (y, placed("c"), pay, other_core(pay), *w_out),
         [pltpu.VMEM((8, TOK, 128), F32)],
-        smem=1,
-    )
-    own = everyone(out, "x")
-    other = lax.ppermute(own, "c", [(0, 1), (1, 0)])
+        smem=2,
+    )
+    own = exchange(out, "x")
+    other = other_core(own)
     hbm = pl.BlockSpec(memory_space=pl.ANY)
     return pl.pallas_call(
         place_kernel,

time: 230 us -> 238 us (1.035)
  blocking collectives: 81.7 us -> 97.4 us
  starting transfers between devices: 81.8 us -> 76.3 us
  local copies, waits for them, and re-layouts: 11.4 us -> 8.54 us
    all_to_all x4 -> x1, starting transfers between devices: 40 us -> 4.33 us  [everyone(): return lax.all_to_all(copies, axis, split_axis=0, concat_axis=0, tiled=True)]
    all_to_all x0 -> x2, blocking collectives: none -> 27 us  [exchange(): return lax.all_to_all(copies, axis, split_axis=0, concat_axis=0, tiled=True)]
    all_to_all x0 -> x2, starting transfers between devices: none -> 21.8 us  [exchange(): return lax.all_to_all(copies, axis, split_axis=0, concat_axis=0, tiled=True)]
    all_to_all x2 -> x1, blocking collectives: 44.9 us -> 33.6 us  [everyone(): return lax.all_to_all(copies, axis, split_axis=0, concat_axis=0, tiled=True)]
    ppermute x1 -> x2, starting transfers between devices: 4.56 us -> 13.1 us  [other_core(): return lax.ppermute(x, 'c', [(0, 1), (1, 0)])]
    broadcast_in_dim x6 -> x2, local copies, waits for them, and re-layouts: 4.2 us -> 1.39 us  [everyone(): copies = jnp.broadcast_to(x, (size, *x.shape))]
    all_to_all x4 -> x1, waiting for transfers between devices: 8.68 us -> 8.67 us  [everyone(): return lax.all_to_all(copies, axis, split_axis=0, concat_axis=0, tiled=True)]
where the time goes in v2:
time: 238 us; the launch traced here: 237 us
  blocking collectives  97.4 us (41%)
  starting transfers between devices  76.3 us (32%)
  waiting for transfers between devices  33.4 us (14%)
  Pallas kernels  19.6 us (8%)
  local copies, waits for them, and re-layouts  8.54 us (4%)
    all_gather x1, blocking collectives, layer(): rest = lax.all_gather(rest, Z)  36.7 us
    all_to_all x1, blocking collectives, everyone(): return lax.all_to_all(copies, axis, split_axis=0, concat_axis=0, tiled=True)  33.6 us
    all_to_all x2, blocking collectives, exchange(): return lax.all_to_all(copies, axis, split_axis=0, concat_axis=0, tiled=True)  27 us
    ppermute x6, starting transfers between devices, neighbours(): pieces.append(lax.ppermute(x, 'y', [(i, (i + k) % 4) for i in range(4)]))  22.8 us
    all_to_all x2, starting transfers between devices, exchange(): return lax.all_to_all(copies, axis, split_axis=0, concat_axis=0, tiled=True)  21.8 us
    pallas_call x6, Pallas kernels, call(): pl.pallas_call(kernel, out_shape=[jax.ShapeDtypeStruct(s, d) for s, d in...  17.4 us
    ppermute x6, waiting for transfers between devices, neighbours(): pieces.append(lax.ppermute(x, 'y', [(i, (i + k) % 4) for i in range(4)]))  16.7 us
    ppermute x2, starting transfers between devices, other_core(): return lax.ppermute(x, 'c', [(0, 1), (1, 0)])  13.1 us
  transfers between devices with their start and end apart: 13, of which 9 were waited for; matrix products, arithmetic and copies ran while one was open for 1% of the time, Pallas kernels for 2%

profile of v2, /device:TPU:1, one launch (start us, length us, event | category | flops | bytes accessed | tf_op | source)
XLA Modules:
  0.0 236.5 jit_solution(16512555856689284542)
XLA Ops:
  0.8 33.6 %all_to_all.30 = bf16[16,32,384]{2,1,0:T(8,128)(2,1)S(1)} all-to-all(bf16[16,32,384]{2,1,0:T(8,128)(2,1)S(1)} %broadcast_in_dim.6), channel_id=1, replica_groups=mesh['za'=4,'zb'=2,'zc'=2,'y'=4,'x'=4,'c'=2] {'za','zb','zc'}, dimensions={0} | all-to-all | bytes 786432 | tf_op jit(solution)/shard_map/all_to_all | solution.py:360
  35.8 4.3 %all-to-all-start.1 = ((bf16[4,16,32,384]{3,2,1,0:T(8,128)(2,1)}), bf16[4,16,32,384]{3,2,1,0:T(8,128)(2,1)S(1)}, u32[]{:S(2)}, u32[]{:S(2)}) async-start(bf16[4,16,32,384]{3,2,1,0:T(8,128)(2,1)} %broadcast_in_dim.7), calls=%async_computation.1 | async-start | bytes 3145728 | tf_op jit(solution)/shard_map/all_to_all | solution.py:360
  45.1 8.7 %all-to-all-done.1.w = bf16[4,16,32,384]{3,2,1,0:T(8,128)(2,1)S(1)} async-done(((bf16[4,16,32,384]{3,2,1,0:T(8,128)(2,1)}), bf16[4,16,32,384]{3,2,1,0:T(8,128)(2,1)S(1)}, u32[]{:S(2)}, u32[]{:S(2)}) %all-to-all-start.1) | async-done | bytes 1572896 | tf_op jit(solution)/shard_map/all_to_all | solution.py:360
  54.8 6.3 %shard_map.191 = (f32[2,256,128]{2,1,0:T(8,128)S(1)}, bf16[8,128,128]{2,1,0:T(8,128)(2,1)}) custom-call(bf16[256,2048]{1,0:T(8,128)(2,1)S(1)} %get-tuple-element.11.x, bf16[4,16,32,384]{3,2,1,0:T(8,128)(2,1)S(1)} %all-to-all-done.1.w, f32[3,256,128]{2,1,0:T(8,128)S(1)} %copy-done.4), custom_call_target="tpu_custom_call" | custom-call | tf_op jit(solution)/shard_map/pallas_call | solution.py:347
  61.1 11.1 %all-to-all-start.2 = ((bf16[8,128,128]{2,1,0:T(8,128)(2,1)}), bf16[8,128,128]{2,1,0:T(8,128)(2,1)S(1)}, u32[]{:S(2)}, u32[]{:S(2)}) async-start(bf16[8,128,128]{2,1,0:T(8,128)(2,1)} %get-tuple-element.13), calls=%async_computation.2 | async-start | bytes 524288 | tf_op jit(solution)/shard_map/all_to_all | solution.py:364
  72.2 12.3 %collective-permute-start.1 = (bf16[32,384]{1,0:T(8,128)(2,1)S(1)}, bf16[32,384]{1,0:T(8,128)(2,1)S(1)}, u32[]{:S(2)}, u32[]{:S(2)}) collective-permute-start(bf16[32,384]{1,0:T(8,128)(2,1)S(1)} %pad_maximum_fusion.2), channel_id=1, source_target_pairs={{0,0},{1,256},{2,8},{3,264},{4,16},{5,272},{6,24},{7,280},{8,32},{... | collective-permute-start | bytes 73736 | tf_op jit(solution)/shard_map/ppermute | solution.py:416
  87.0 10.7 %all-to-all-start.3 = ((bf16[8,128,128]{2,1,0:T(8,128)(2,1)}), bf16[8,128,128]{2,1,0:T(8,128)(2,1)S(1)}, u32[]{:S(2)}, u32[]{:S(2)}) async-start(bf16[8,128,128]{2,1,0:T(8,128)(2,1)} %get-tuple-element.14), calls=%async_computation.3 | async-start | bytes 524288 | tf_op jit(solution)/shard_map/all_to_all | solution.py:364
  97.7 36.7 %all-gather = bf16[512,896]{1,0:T(8,128)(2,1)S(1)} all-gather(bf16[32,896]{1,0:T(8,128)(2,1)S(1)} %pad_maximum_fusion), channel_id=2, replica_groups=mesh['za'=4,'zb'=2,'zc'=2,'y'=4,'x'=4,'c'=2] {'za','zb','zc'}, dimensions={0}, use_global_device_ids=true | all-gather | bytes 974848 | tf_op jit(solution)/shard_map/all_gather | solution.py:418
  134.5 3.3 %collective-permute-start.2 = (bf16[16,32,512]{2,1,0:T(8,128)(2,1)S(1)}, bf16[16,32,512]{2,1,0:T(8,128)(2,1)S(1)}, u32[]{:S(2)}, u32[]{:S(2)}) collective-permute-start(bf16[16,32,512]{2,1,0:T(8,128)(2,1)S(1)} %slice.12.w0), channel_id=1, source_target_pairs={{0,8},{8,16},{16,24},{24,0},{1,9},{9,17},{17,25},{25,1},{2,10},{10... | collective-permute-start | bytes 1572872 | tf_op jit(solution)/shard_map/ppermute | solution.py:378
  137.8 5.9 %collective-permute-start.3 = (bf16[16,32,512]{2,1,0:T(8,128)(2,1)S(1)}, bf16[16,32,512]{2,1,0:T(8,128)(2,1)S(1)}, u32[]{:S(2)}, u32[]{:S(2)}) collective-permute-start(bf16[16,32,512]{2,1,0:T(8,128)(2,1)S(1)} %slice.12.w0), channel_id=1, source_target_pairs={{0,16},{8,24},{16,0},{24,8},{1,17},{9,25},{17,1},{25,9},{2,18},{10... | collective-permute-start | bytes 1572872 | tf_op jit(solution)/shard_map/ppermute | solution.py:378
  143.7 3.4 %collective-permute-start.4 = (bf16[16,32,512]{2,1,0:T(8,128)(2,1)S(1)}, bf16[16,32,512]{2,1,0:T(8,128)(2,1)}, u32[]{:S(2)}, u32[]{:S(2)}) collective-permute-start(bf16[16,32,512]{2,1,0:T(8,128)(2,1)S(1)} %slice.12.w0), channel_id=1, source_target_pairs={{0,24},{8,0},{16,8},{24,16},{1,25},{9,1},{17,9},{25,17},{2,26},{10... | collective-permute-start | bytes 1572872 | tf_op jit(solution)/shard_map/ppermute | solution.py:378
  150.0 5.6 %collective-permute-done.halo = bf16[32,2048]{1,0:T(8,128)(2,1)S(1)} collective-permute-done((bf16[32,2048]{1,0:T(8,128)(2,1)S(1)}, bf16[32,2048]{1,0:T(8,128)(2,1)S(1)}, u32[]{:S(2)}, u32[]{:S(2)}) %collective-permute-start) | collective-permute-done | bytes 131104 | tf_op jit(solution)/shard_map/ppermute | solution.py:409
  157.9 3.9 %shard_map.193.dev = bf16[272,256]{1,0:T(8,128)(2,1)S(1)} custom-call(s32[1]{0:T(128)} %bitcast.1.place, bf16[256,2048]{1,0:T(8,128)(2,1)S(1)} %get-tuple-element.11.x, bf16[32,2048]{1,0:T(8,128)(2,1)S(1)} %collective-permute-done.halo, f32[1,2048]{1,0:T(1,128)S(1)} %bitcast.11, bf16[16,32,512]{2,1,0:T(8,128)(2,1)S(1)} %slice.12.w0, ...), custom_call_target="tpu_custom_call" | custom-call | tf_op jit(solution)/shard_map/pallas_call | solution.py:347
  163.1 16.2 %all_to_all.31.own = bf16[4,400,256]{2,1,0:T(8,128)(2,1)S(1)} all-to-all(bf16[4,400,256]{2,1,0:T(8,128)(2,1)S(1)} %shard_map.194), channel_id=1, replica_groups=mesh['za'=4,'zb'=2,'zc'=2,'y'=4,'x'=4,'c'=2] {'x'}, dimensions={0} | all-to-all | bytes 1638400 | tf_op jit(solution)/shard_map/all_to_all | solution.py:364
  179.2 9.2 %collective-permute-start.5 = (bf16[4,400,256]{2,1,0:T(8,128)(2,1)S(1)}, bf16[4,400,256]{2,1,0:T(8,128)(2,1)S(1)}, u32[]{:S(2)}, u32[]{:S(2)}) collective-permute-start(bf16[4,400,256]{2,1,0:T(8,128)(2,1)S(1)} %all_to_all.31.own), channel_id=1, source_target_pairs={{0,1},{1,0},{2,3},{3,2},{4,5},{5,4},{6,7},{7,6},{8,9},{9,8},{10,11... | collective-permute-start | bytes 2457608 | tf_op jit(solution)/shard_map/ppermute | solution.py:368
  189.5 3.5 %collective-permute-start.6 = (bf16[16,32,384]{2,1,0:T(8,128)(2,1)S(1)}, bf16[16,32,384]{2,1,0:T(8,128)(2,1)S(1)}, u32[]{:S(2)}, u32[]{:S(2)}) collective-permute-start(bf16[16,32,384]{2,1,0:T(8,128)(2,1)S(1)} %slice.13.w0), channel_id=1, source_target_pairs={{0,8},{8,16},{16,24},{24,0},{1,9},{9,17},{17,25},{25,1},{2,10},{10... | collective-permute-start | bytes 1179656 | tf_op jit(solution)/shard_map/ppermute | solution.py:378
  193.0 4.0 %collective-permute-start.7 = (bf16[16,32,384]{2,1,0:T(8,128)(2,1)S(1)}, bf16[16,32,384]{2,1,0:T(8,128)(2,1)S(1)}, u32[]{:S(2)}, u32[]{:S(2)}) collective-permute-start(bf16[16,32,384]{2,1,0:T(8,128)(2,1)S(1)} %slice.13.w0), channel_id=1, source_target_pairs={{0,16},{8,24},{16,0},{24,8},{1,17},{9,25},{17,1},{25,9},{2,18},{10... | collective-permute-start | bytes 1179656 | tf_op jit(solution)/shard_map/ppermute | solution.py:378
  197.0 2.6 %collective-permute-start.8 = (bf16[16,32,384]{2,1,0:T(8,128)(2,1)S(1)}, bf16[16,32,384]{2,1,0:T(8,128)(2,1)S(1)}, u32[]{:S(2)}, u32[]{:S(2)}) collective-permute-start(bf16[16,32,384]{2,1,0:T(8,128)(2,1)S(1)} %slice.13.w0), channel_id=1, source_target_pairs={{0,24},{8,0},{16,8},{24,16},{1,25},{9,1},{17,9},{25,17},{2,26},{10... | collective-permute-start | bytes 1179656 | tf_op jit(solution)/shard_map/ppermute | solution.py:378
  199.7 3.6 %collective-permute-done.6.w1 = bf16[16,32,384]{2,1,0:T(8,128)(2,1)S(1)} collective-permute-done((bf16[16,32,384]{2,1,0:T(8,128)(2,1)S(1)}, bf16[16,32,384]{2,1,0:T(8,128)(2,1)S(1)}, u32[]{:S(2)}, u32[]{:S(2)}) %collective-permute-start.6) | collective-permute-done | bytes 393248 | tf_op jit(solution)/shard_map/ppermute | solution.py:378
  203.3 9.2 %collective-permute-done.7.w2 = bf16[16,32,384]{2,1,0:T(8,128)(2,1)S(1)} collective-permute-done((bf16[16,32,384]{2,1,0:T(8,128)(2,1)S(1)}, bf16[16,32,384]{2,1,0:T(8,128)(2,1)S(1)}, u32[]{:S(2)}, u32[]{:S(2)}) %collective-permute-start.7) | collective-permute-done | bytes 393248 | tf_op jit(solution)/shard_map/ppermute | solution.py:378
  214.2 2.9 %shard_map.195 = bf16[4,256,256]{2,1,0:T(8,128)(2,1)S(1)} custom-call(s32[1]{0:T(128)} %bitcast.1.place, s32[1]{0:T(128)} %bitcast.core.place, bf16[4,400,256]{2,1,0:T(8,128)(2,1)S(1)} %all_to_all.31.own, bf16[4,400,256]{2,1,0:T(8,128)(2,1)S(1)} %collective-permute-done.5.other, bf16[16,32,384]{2,1,0:T(8,128)(2,1)S(1)} %slice.13.w0, ...), custom_call_target="tpu_custom_call" | custom-call | tf_op jit(solution)/shard_map/pallas_call | solution.py:347
  217.1 10.8 %all_to_all.32.own = bf16[4,256,256]{2,1,0:T(8,128)(2,1)S(1)} all-to-all(bf16[4,256,256]{2,1,0:T(8,128)(2,1)S(1)} %shard_map.195), channel_id=1, replica_groups=mesh['za'=4,'zb'=2,'zc'=2,'y'=4,'x'=4,'c'=2] {'x'}, dimensions={0} | all-to-all | bytes 1048576 | tf_op jit(solution)/shard_map/all_to_all | solution.py:364
  227.9 3.9 %collective-permute-start.9 = (bf16[4,256,256]{2,1,0:T(8,128)(2,1)S(1)}, bf16[4,256,256]{2,1,0:T(8,128)(2,1)S(1)}, u32[]{:S(2)}, u32[]{:S(2)}) collective-permute-start(bf16[4,256,256]{2,1,0:T(8,128)(2,1)S(1)} %all_to_all.32.own), channel_id=1, source_target_pairs={{0,1},{1,0},{2,3},{3,2},{4,5},{5,4},{6,7},{7,6},{8,9},{9,8},{10,11... | collective-permute-start | bytes 1572872 | tf_op jit(solution)/shard_map/ppermute | solution.py:368
  234.1 2.2 place.1
  (67 shorter events, 21.8 us)
Async XLA Ops:
  35.8 4.7 %copy-start.6 = (bf16[128,128]{1,0:T(8,128)(2,1)S(1)}, bf16[128,128]{1,0:T(8,128)(2,1)}, u32[]{:S(2)}) copy-start(bf16[128,128]{1,0:T(8,128)(2,1)} %ls.1) | copy-start | bytes 98308
  35.8 4.7 %copy-start.8 = (f32[2048]{0:T(1024)S(1)}, f32[2048]{0:T(1024)}, u32[]{:S(2)}) copy-start(f32[2048]{0:T(1024)} %param.21) | copy-start | bytes 24580
  35.8 4.7 %copy-start.10 = (f32[128]{0:T(128)S(1)}, f32[128]{0:T(128)}, u32[]{:S(2)}) copy-start(f32[128]{0:T(128)} %param.27) | copy-start | bytes 1540
  35.8 17.9 %all-to-all-start.1 = ((bf16[4,16,32,384]{3,2,1,0:T(8,128)(2,1)}), bf16[4,16,32,384]{3,2,1,0:T(8,128)(2,1)S(1)}, u32[]{:S(2)}, u32[]{:S(2)}) async-start(bf16[4,16,32,384]{3,2,1,0:T(8,128)(2,1)} %broadcast_in_dim.7), calls=%async_computation.1 | async-start | bytes 3145728 | tf_op jit(solution)/shard_map/all_to_all | solution.py:360
  54.7 17.4 %copy-start.16 = (bf16[32,256]{1,0:T(8,128)(2,1)S(1)}, bf16[32,256]{1,0:T(8,128)(2,1)}, u32[]{:S(2)}) copy-start(bf16[32,256]{1,0:T(8,128)(2,1)} %param.39) | copy-start | bytes 49156
  54.8 17.4 %copy-start.19 = (bf16[32,128]{1,0:T(8,128)(2,1)S(1)}, bf16[32,128]{1,0:T(8,128)(2,1)}, u32[]{:S(2)}) copy-start(bf16[32,128]{1,0:T(8,128)(2,1)} %param.38) | copy-start | bytes 24580
  54.8 30.7 %copy-start.17 = (bf16[32,256]{1,0:T(8,128)(2,1)S(1)}, bf16[32,256]{1,0:T(8,128)(2,1)}, u32[]{:S(2)}) copy-start(bf16[32,256]{1,0:T(8,128)(2,1)} %param.26) | copy-start | bytes 49156
  54.8 30.7 %copy-start.18 = (bf16[32,256]{1,0:T(8,128)(2,1)S(1)}, bf16[32,256]{1,0:T(8,128)(2,1)}, u32[]{:S(2)}) copy-start(bf16[32,256]{1,0:T(8,128)(2,1)} %param.25) | copy-start | bytes 49156
  61.1 24.4 %all-to-all-start.2 = ((bf16[8,128,128]{2,1,0:T(8,128)(2,1)}), bf16[8,128,128]{2,1,0:T(8,128)(2,1)S(1)}, u32[]{:S(2)}, u32[]{:S(2)}) async-start(bf16[8,128,128]{2,1,0:T(8,128)(2,1)} %get-tuple-element.13), calls=%async_computation.2 | async-start | bytes 524288 | tf_op jit(solution)/shard_map/all_to_all | solution.py:364
  72.2 13.2 %collective-permute-start.1 = (bf16[32,384]{1,0:T(8,128)(2,1)S(1)}, bf16[32,384]{1,0:T(8,128)(2,1)S(1)}, u32[]{:S(2)}, u32[]{:S(2)}) collective-permute-start(bf16[32,384]{1,0:T(8,128)(2,1)S(1)} %pad_maximum_fusion.2), channel_id=1, source_target_pairs={{0,0},{1,256},{2,8},{3,264},{4,16},{5,272},{6,24},{7,280},{8,32},{... | collective-permute-start | bytes 73736 | tf_op jit(solution)/shard_map/ppermute | solution.py:416
  85.5 72.4 %copy-start.7 = (f32[31,256]{1,0:T(8,128)S(1)}, f32[31,256]{1,0:T(8,128)}, u32[]{:S(2)}) copy-start(f32[31,256]{1,0:T(8,128)} %taps.1) | copy-start | bytes 95236
  85.5 72.4 %copy-start.9 = (f32[256]{0:T(256)S(1)}, f32[256]{0:T(256)}, u32[]{:S(2)}) copy-start(f32[256]{0:T(256)} %param.37) | copy-start | bytes 3076
  87.0 74.8 %all-to-all-start.3 = ((bf16[8,128,128]{2,1,0:T(8,128)(2,1)}), bf16[8,128,128]{2,1,0:T(8,128)(2,1)S(1)}, u32[]{:S(2)}, u32[]{:S(2)}) async-start(bf16[8,128,128]{2,1,0:T(8,128)(2,1)} %get-tuple-element.14), calls=%async_computation.3 | async-start | bytes 524288 | tf_op jit(solution)/shard_map/all_to_all | solution.py:364
  134.4 12.7 %copy-start.13 = (bf16[512,896]{1,0:T(8,128)(2,1)}, bf16[512,896]{1,0:T(8,128)(2,1)S(1)}, u32[]{:S(2)}) copy-start(bf16[512,896]{1,0:T(8,128)(2,1)S(1)} %all-gather) | copy-start | bytes 2752516
  134.5 21.1 %collective-permute-start.2 = (bf16[16,32,512]{2,1,0:T(8,128)(2,1)S(1)}, bf16[16,32,512]{2,1,0:T(8,128)(2,1)S(1)}, u32[]{:S(2)}, u32[]{:S(2)}) collective-permute-start(bf16[16,32,512]{2,1,0:T(8,128)(2,1)S(1)} %slice.12.w0), channel_id=1, source_target_pairs={{0,8},{8,16},{16,24},{24,0},{1,9},{9,17},{17,25},{25,1},{2,10},{10... | collective-permute-start | bytes 1572872 | tf_op jit(solution)/shard_map/ppermute | solution.py:378
  137.8 18.4 %collective-permute-start.3 = (bf16[16,32,512]{2,1,0:T(8,128)(2,1)S(1)}, bf16[16,32,512]{2,1,0:T(8,128)(2,1)S(1)}, u32[]{:S(2)}, u32[]{:S(2)}) collective-permute-start(bf16[16,32,512]{2,1,0:T(8,128)(2,1)S(1)} %slice.12.w0), channel_id=1, source_target_pairs={{0,16},{8,24},{16,0},{24,8},{1,17},{9,25},{17,1},{25,9},{2,18},{10... | collective-permute-start | bytes 1572872 | tf_op jit(solution)/shard_map/ppermute | solution.py:378
  143.7 14.1 %collective-permute-start.4 = (bf16[16,32,512]{2,1,0:T(8,128)(2,1)S(1)}, bf16[16,32,512]{2,1,0:T(8,128)(2,1)}, u32[]{:S(2)}, u32[]{:S(2)}) collective-permute-start(bf16[16,32,512]{2,1,0:T(8,128)(2,1)S(1)} %slice.12.w0), channel_id=1, source_target_pairs={{0,24},{8,0},{16,8},{24,16},{1,25},{9,1},{17,9},{25,17},{2,26},{10... | collective-permute-start | bytes 1572872 | tf_op jit(solution)/shard_map/ppermute | solution.py:378
  148.1 7.5 %collective-permute-start = (bf16[32,2048]{1,0:T(8,128)(2,1)S(1)}, bf16[32,2048]{1,0:T(8,128)(2,1)S(1)}, u32[]{:S(2)}, u32[]{:S(2)}) collective-permute-start(bf16[32,2048]{1,0:T(8,128)(2,1)S(1)} %slice.9), channel_id=1, source_target_pairs={{0,8},{8,16},{16,24},{24,32},{32,40},{40,48},{48,56},{56,64},{64,7... | collective-permute-start | bytes 393224 | tf_op jit(solution)/shard_map/ppermute | solution.py:409
  179.2 34.9 %collective-permute-start.5 = (bf16[4,400,256]{2,1,0:T(8,128)(2,1)S(1)}, bf16[4,400,256]{2,1,0:T(8,128)(2,1)S(1)}, u32[]{:S(2)}, u32[]{:S(2)}) collective-permute-start(bf16[4,400,256]{2,1,0:T(8,128)(2,1)S(1)} %all_to_all.31.own), channel_id=1, source_target_pairs={{0,1},{1,0},{2,3},{3,2},{4,5},{5,4},{6,7},{7,6},{8,9},{9,8},{10,11... | collective-permute-start | bytes 2457608 | tf_op jit(solution)/shard_map/ppermute | solution.py:368
  189.5 13.8 %collective-permute-start.6 = (bf16[16,32,384]{2,1,0:T(8,128)(2,1)S(1)}, bf16[16,32,384]{2,1,0:T(8,128)(2,1)S(1)}, u32[]{:S(2)}, u32[]{:S(2)}) collective-permute-start(bf16[16,32,384]{2,1,0:T(8,128)(2,1)S(1)} %slice.13.w0), channel_id=1, source_target_pairs={{0,8},{8,16},{16,24},{24,0},{1,9},{9,17},{17,25},{25,1},{2,10},{10... | collective-permute-start | bytes 1179656 | tf_op jit(solution)/shard_map/ppermute | solution.py:378
  193.0 19.5 %collective-permute-start.7 = (bf16[16,32,384]{2,1,0:T(8,128)(2,1)S(1)}, bf16[16,32,384]{2,1,0:T(8,128)(2,1)S(1)}, u32[]{:S(2)}, u32[]{:S(2)}) collective-permute-start(bf16[16,32,384]{2,1,0:T(8,128)(2,1)S(1)} %slice.13.w0), channel_id=1, source_target_pairs={{0,16},{8,24},{16,0},{24,8},{1,17},{9,25},{17,1},{25,9},{2,18},{10... | collective-permute-start | bytes 1179656 | tf_op jit(solution)/shard_map/ppermute | solution.py:378
  197.0 17.1 %collective-permute-start.8 = (bf16[16,32,384]{2,1,0:T(8,128)(2,1)S(1)}, bf16[16,32,384]{2,1,0:T(8,128)(2,1)S(1)}, u32[]{:S(2)}, u32[]{:S(2)}) collective-permute-start(bf16[16,32,384]{2,1,0:T(8,128)(2,1)S(1)} %slice.13.w0), channel_id=1, source_target_pairs={{0,24},{8,0},{16,8},{24,16},{1,25},{9,1},{17,9},{25,17},{2,26},{10... | collective-permute-start | bytes 1179656 | tf_op jit(solution)/shard_map/ppermute | solution.py:378
  227.9 5.4 %copy-start.14 = (bf16[4,256,256]{2,1,0:T(8,128)(2,1)}, bf16[4,256,256]{2,1,0:T(8,128)(2,1)S(1)}, u32[]{:S(2)}) copy-start(bf16[4,256,256]{2,1,0:T(8,128)(2,1)S(1)} %all_to_all.32.own) | copy-start | bytes 1572868
  227.9 5.4 %collective-permute-start.9 = (bf16[4,256,256]{2,1,0:T(8,128)(2,1)S(1)}, bf16[4,256,256]{2,1,0:T(8,128)(2,1)S(1)}, u32[]{:S(2)}, u32[]{:S(2)}) collective-permute-start(bf16[4,256,256]{2,1,0:T(8,128)(2,1)S(1)} %all_to_all.32.own), channel_id=1, source_target_pairs={{0,1},{1,0},{2,3},{3,2},{4,5},{5,4},{6,7},{7,6},{8,9},{9,8},{10,11... | collective-permute-start | bytes 1572872 | tf_op jit(solution)/shard_map/ppermute | solution.py:368
  (11 other events, 31.7 us)

commit v3 on v2

--- a/solution.py
+++ b/solution.py
@@ -15,8 +15,8 @@
 SP = ("za", "zb", "zc", "y")
 Z = ("za", "zb", "zc")
 TP = ("x", "c")
-FAR = ("za", "zb")
-NEAR = ("zc", "y")
+FAR = "za"
+NEAR = ("zb", "zc", "y")
 RMS_EPSILON = 1e-06
 GROUP_EPSILON = 0.00064
 LAYER_EPSILON = 1e-05
@@ -192,7 +192,7 @@
     dpart = jnp.where(half, zs[0][:64], zs[1][:64]) + jnp.where(diag, jnp.exp(last) - 1.0, 0.0)
     ppart = jnp.where(half, zs[0][64:] + vk[:64], zs[1][64:] + vk[64:])
     mine = jnp.concatenate([dpart, ppart], axis=0).astype(BF)
-    for k in range(8):
+    for k in range(16):
         trans[k] = mine
 
 
@@ -215,11 +215,11 @@
 
 
 def unpacked(ref):
-    return [(ref[k, :64].astype(F32), ref[k, 64:].astype(F32)) for k in range(8)]
+    return [(ref[k, :64].astype(F32), ref[k, 64:].astype(F32)) for k in range(ref.shape[0])]
 
 
 def passed(place, pieces):
-    keep = [place[0] > k for k in range(8)]
+    keep = [place[0] > k for k in range(len(pieces))]
     return [(jnp.where(on, d, 0.0), jnp.where(on, p, 0.0)) for on, (d, p) in zip(keep, pieces)]
 
 
@@ -227,7 +227,7 @@
     each = unpacked(pieces)
     d, p = fold(each)
     d, p = d.astype(BF), p.astype(BF)
-    for k in range(8):
+    for k in range(4):
         total[k, :64] = d
         total[k, 64:] = p
     d, p = fold(passed(place, each))
@@ -438,14 +438,14 @@
     square = pltpu.VMEM((2, TOK, TOK), F32)
     parts, trans = call(
         state_kernel,
-        [((2, TOK, 128), F32), ((8, 128, 128), BF)],
+        [((2, TOK, 128), F32), ((16, 128, 128), BF)],
         (normed, w_state, rates),
         [pltpu.VMEM((16, 4, 32, 384), BF), pltpu.VMEM((2, TOK, TOK), BF), square, square, square],
     )
 
     total, before = call(
         prefix_kernel,
-        [((8, 128, 128), BF), ((128, 128), F32)],
+        [((4, 128, 128), BF), ((128, 128), F32)],
         (placed(NEAR), exchange(trans, NEAR)),
         smem=1,
     )

time: 238 us -> 230 us (0.966)
  blocking collectives: 97.4 us -> 88 us
    all_gather x1, blocking collectives: 36.7 us -> 28.5 us  [layer(): rest = lax.all_gather(rest, Z)]
    ppermute x2, starting transfers between devices: 13.1 us -> 17.3 us  [other_core(): return lax.ppermute(x, 'c', [(0, 1), (1, 0)])]
    ppermute x1, waiting for transfers between devices: 0.92 us -> 4.79 us  [layer(): w_out = lax.ppermute(w_out, (*SP, *TP), moves)]
    ppermute x6, starting transfers between devices: 22.8 us -> 19.5 us  [neighbours(): pieces.append(lax.ppermute(x, 'y', [(i, (i + k) % 4) for i in range(4)]))]
    ppermute x1, waiting for transfers between devices: 5.61 us -> 3.1 us  [layer(): lax.ppermute(tokens[TOK - HALO:], SP, [(i, i + 1) for i in range(63)])]
  transfers between devices with their start and end apart: 13 -> 13, of which waited for: 9 -> 8; matrix products, arithmetic and copies ran while one was open for 1% -> 1% of each run, Pallas kernels for 2% -> 3%
where the time goes in v3:
time: 230 us; the launch traced here: 229 us
  blocking collectives  88 us (38%)
  starting transfers between devices  75.2 us (33%)
  waiting for transfers between devices  35 us (15%)
  Pallas kernels  20.1 us (9%)
  local copies, waits for them, and re-layouts  9.46 us (4%)
    all_to_all x1, blocking collectives, everyone(): return lax.all_to_all(copies, axis, split_axis=0, concat_axis=0, tiled=True)  33.6 us
    all_gather x1, blocking collectives, layer(): rest = lax.all_gather(rest, Z)  28.5 us
    all_to_all x2, blocking collectives, exchange(): return lax.all_to_all(copies, axis, split_axis=0, concat_axis=0, tiled=True)  25.9 us
    all_to_all x2, starting transfers between devices, exchange(): return lax.all_to_all(copies, axis, split_axis=0, concat_axis=0, tiled=True)  20.3 us
    ppermute x6, starting transfers between devices, neighbours(): pieces.append(lax.ppermute(x, 'y', [(i, (i + k) % 4) for i in range(4)]))  19.5 us
    pallas_call x6, Pallas kernels, call(): pl.pallas_call(kernel, out_shape=[jax.ShapeDtypeStruct(s, d) for s, d in...  17.9 us
    ppermute x2, starting transfers between devices, other_core(): return lax.ppermute(x, 'c', [(0, 1), (1, 0)])  17.3 us
    ppermute x6, waiting for transfers between devices, neighbours(): pieces.append(lax.ppermute(x, 'y', [(i, (i + k) % 4) for i in range(4)]))  15.5 us
  transfers between devices with their start and end apart: 13, of which 8 were waited for; matrix products, arithmetic and copies ran while one was open for 1% of the time, Pallas kernels for 3%

profile of v3, /device:TPU:1, one launch (start us, length us, event | category | flops | bytes accessed | tf_op | source)
XLA Modules:
  0.0 229.1 jit_solution(18301767068659733633)
XLA Ops:
  0.8 33.6 %all_to_all.30 = bf16[16,32,384]{2,1,0:T(8,128)(2,1)S(1)} all-to-all(bf16[16,32,384]{2,1,0:T(8,128)(2,1)S(1)} %broadcast_in_dim.6), channel_id=1, replica_groups=mesh['za'=4,'zb'=2,'zc'=2,'y'=4,'x'=4,'c'=2] {'za','zb','zc'}, dimensions={0} | all-to-all | bytes 786432 | tf_op jit(solution)/shard_map/all_to_all | solution.py:360
  35.8 4.3 %all-to-all-start.1 = ((bf16[4,16,32,384]{3,2,1,0:T(8,128)(2,1)}), bf16[4,16,32,384]{3,2,1,0:T(8,128)(2,1)S(1)}, u32[]{:S(2)}, u32[]{:S(2)}) async-start(bf16[4,16,32,384]{3,2,1,0:T(8,128)(2,1)} %broadcast_in_dim.7), calls=%async_computation.1 | async-start | bytes 3145728 | tf_op jit(solution)/shard_map/all_to_all | solution.py:360
  45.1 8.7 %all-to-all-done.1.w = bf16[4,16,32,384]{3,2,1,0:T(8,128)(2,1)S(1)} async-done(((bf16[4,16,32,384]{3,2,1,0:T(8,128)(2,1)}), bf16[4,16,32,384]{3,2,1,0:T(8,128)(2,1)S(1)}, u32[]{:S(2)}, u32[]{:S(2)}) %all-to-all-start.1) | async-done | bytes 1572896 | tf_op jit(solution)/shard_map/all_to_all | solution.py:360
  54.8 6.5 %shard_map.191 = (f32[2,256,128]{2,1,0:T(8,128)S(1)}, bf16[16,128,128]{2,1,0:T(8,128)(2,1)}) custom-call(bf16[256,2048]{1,0:T(8,128)(2,1)S(1)} %get-tuple-element.11.x, bf16[4,16,32,384]{3,2,1,0:T(8,128)(2,1)S(1)} %all-to-all-done.1.w, f32[3,256,128]{2,1,0:T(8,128)S(1)} %copy-done.4), custom_call_target="tpu_custom_call" | custom-call | tf_op jit(solution)/shard_map/pallas_call | solution.py:347
  61.2 13.4 %all-to-all-start.2 = ((bf16[16,128,128]{2,1,0:T(8,128)(2,1)}), bf16[16,128,128]{2,1,0:T(8,128)(2,1)S(1)}, u32[]{:S(2)}, u32[]{:S(2)}) async-start(bf16[16,128,128]{2,1,0:T(8,128)(2,1)} %get-tuple-element.13), calls=%async_computation.2 | async-start | bytes 1048576 | tf_op jit(solution)/shard_map/all_to_all | solution.py:364
  74.7 10.9 %collective-permute-start.1 = (bf16[32,384]{1,0:T(8,128)(2,1)S(1)}, bf16[32,384]{1,0:T(8,128)(2,1)S(1)}, u32[]{:S(2)}, u32[]{:S(2)}) collective-permute-start(bf16[32,384]{1,0:T(8,128)(2,1)S(1)} %pad_maximum_fusion.2), channel_id=1, source_target_pairs={{0,0},{1,256},{2,8},{3,264},{4,16},{5,272},{6,24},{7,280},{8,32},{... | collective-permute-start | bytes 73736 | tf_op jit(solution)/shard_map/ppermute | solution.py:416
  85.6 4.8 %collective-permute-done.1 = bf16[32,384]{1,0:T(8,128)(2,1)S(1)} collective-permute-done((bf16[32,384]{1,0:T(8,128)(2,1)S(1)}, bf16[32,384]{1,0:T(8,128)(2,1)S(1)}, u32[]{:S(2)}, u32[]{:S(2)}) %collective-permute-start.1) | collective-permute-done | bytes 24608 | tf_op jit(solution)/shard_map/ppermute | solution.py:416
  90.4 28.5 %all-gather = bf16[512,896]{1,0:T(8,128)(2,1)S(1)} all-gather(bf16[32,896]{1,0:T(8,128)(2,1)S(1)} %pad_maximum_fusion), channel_id=2, replica_groups=mesh['za'=4,'zb'=2,'zc'=2,'y'=4,'x'=4,'c'=2] {'za','zb','zc'}, dimensions={0}, use_global_device_ids=true | all-gather | bytes 974848 | tf_op jit(solution)/shard_map/all_gather | solution.py:418
  119.9 3.3 %collective-permute-start.2 = (bf16[16,32,512]{2,1,0:T(8,128)(2,1)S(1)}, bf16[16,32,512]{2,1,0:T(8,128)(2,1)S(1)}, u32[]{:S(2)}, u32[]{:S(2)}) collective-permute-start(bf16[16,32,512]{2,1,0:T(8,128)(2,1)S(1)} %slice.12.w0), channel_id=1, source_target_pairs={{0,8},{8,16},{16,24},{24,0},{1,9},{9,17},{17,25},{25,1},{2,10},{10... | collective-permute-start | bytes 1572872 | tf_op jit(solution)/shard_map/ppermute | solution.py:378
  123.2 4.5 %collective-permute-start.3 = (bf16[16,32,512]{2,1,0:T(8,128)(2,1)S(1)}, bf16[16,32,512]{2,1,0:T(8,128)(2,1)S(1)}, u32[]{:S(2)}, u32[]{:S(2)}) collective-permute-start(bf16[16,32,512]{2,1,0:T(8,128)(2,1)S(1)} %slice.12.w0), channel_id=1, source_target_pairs={{0,16},{8,24},{16,0},{24,8},{1,17},{9,25},{17,1},{25,9},{2,18},{10... | collective-permute-start | bytes 1572872 | tf_op jit(solution)/shard_map/ppermute | solution.py:378
  127.7 2.7 %collective-permute-start.4 = (bf16[16,32,512]{2,1,0:T(8,128)(2,1)S(1)}, bf16[16,32,512]{2,1,0:T(8,128)(2,1)}, u32[]{:S(2)}, u32[]{:S(2)}) collective-permute-start(bf16[16,32,512]{2,1,0:T(8,128)(2,1)S(1)} %slice.12.w0), channel_id=1, source_target_pairs={{0,24},{8,0},{16,8},{24,16},{1,25},{9,1},{17,9},{25,17},{2,26},{10... | collective-permute-start | bytes 1572872 | tf_op jit(solution)/shard_map/ppermute | solution.py:378
  132.6 6.9 %all-to-all-start.3 = ((bf16[4,128,128]{2,1,0:T(8,128)(2,1)}), bf16[4,128,128]{2,1,0:T(8,128)(2,1)S(1)}, u32[]{:S(2)}, u32[]{:S(2)}) async-start(bf16[4,128,128]{2,1,0:T(8,128)(2,1)} %get-tuple-element.14), calls=%async_computation.3 | async-start | bytes 262144 | tf_op jit(solution)/shard_map/all_to_all | solution.py:364
  140.4 2.9 %collective-permute-start = (bf16[32,2048]{1,0:T(8,128)(2,1)S(1)}, bf16[32,2048]{1,0:T(8,128)(2,1)S(1)}, u32[]{:S(2)}, u32[]{:S(2)}) collective-permute-start(bf16[32,2048]{1,0:T(8,128)(2,1)S(1)} %slice.9), channel_id=1, source_target_pairs={{0,8},{8,16},{16,24},{24,32},{32,40},{40,48},{48,56},{56,64},{64,7... | collective-permute-start | bytes 393224 | tf_op jit(solution)/shard_map/ppermute | solution.py:409
  143.3 3.1 %collective-permute-done.halo = bf16[32,2048]{1,0:T(8,128)(2,1)S(1)} collective-permute-done((bf16[32,2048]{1,0:T(8,128)(2,1)S(1)}, bf16[32,2048]{1,0:T(8,128)(2,1)S(1)}, u32[]{:S(2)}, u32[]{:S(2)}) %collective-permute-start) | collective-permute-done | bytes 131104 | tf_op jit(solution)/shard_map/ppermute | solution.py:409
  146.5 3.9 %shard_map.193.dev = bf16[272,256]{1,0:T(8,128)(2,1)S(1)} custom-call(s32[1]{0:T(128)} %bitcast.1.place, bf16[256,2048]{1,0:T(8,128)(2,1)S(1)} %get-tuple-element.11.x, bf16[32,2048]{1,0:T(8,128)(2,1)S(1)} %collective-permute-done.halo, f32[1,2048]{1,0:T(1,128)S(1)} %bitcast.11, bf16[16,32,512]{2,1,0:T(8,128)(2,1)S(1)} %slice.12.w0, ...), custom_call_target="tpu_custom_call" | custom-call | tf_op jit(solution)/shard_map/pallas_call | solution.py:347
  152.9 15.1 %all_to_all.31.own = bf16[4,400,256]{2,1,0:T(8,128)(2,1)S(1)} all-to-all(bf16[4,400,256]{2,1,0:T(8,128)(2,1)S(1)} %shard_map.194), channel_id=1, replica_groups=mesh['za'=4,'zb'=2,'zc'=2,'y'=4,'x'=4,'c'=2] {'x'}, dimensions={0} | all-to-all | bytes 1638400 | tf_op jit(solution)/shard_map/all_to_all | solution.py:364
  167.9 13.4 %collective-permute-start.5 = (bf16[4,400,256]{2,1,0:T(8,128)(2,1)S(1)}, bf16[4,400,256]{2,1,0:T(8,128)(2,1)S(1)}, u32[]{:S(2)}, u32[]{:S(2)}) collective-permute-start(bf16[4,400,256]{2,1,0:T(8,128)(2,1)S(1)} %all_to_all.31.own), channel_id=1, source_target_pairs={{0,1},{1,0},{2,3},{3,2},{4,5},{5,4},{6,7},{7,6},{8,9},{9,8},{10,11... | collective-permute-start | bytes 2457608 | tf_op jit(solution)/shard_map/ppermute | solution.py:368
  184.3 4.2 %collective-permute-start.7 = (bf16[16,32,384]{2,1,0:T(8,128)(2,1)S(1)}, bf16[16,32,384]{2,1,0:T(8,128)(2,1)S(1)}, u32[]{:S(2)}, u32[]{:S(2)}) collective-permute-start(bf16[16,32,384]{2,1,0:T(8,128)(2,1)S(1)} %slice.13.w0), channel_id=1, source_target_pairs={{0,16},{8,24},{16,0},{24,8},{1,17},{9,25},{17,1},{25,9},{2,18},{10... | collective-permute-start | bytes 1179656 | tf_op jit(solution)/shard_map/ppermute | solution.py:378
  188.5 2.9 %collective-permute-start.8 = (bf16[16,32,384]{2,1,0:T(8,128)(2,1)S(1)}, bf16[16,32,384]{2,1,0:T(8,128)(2,1)S(1)}, u32[]{:S(2)}, u32[]{:S(2)}) collective-permute-start(bf16[16,32,384]{2,1,0:T(8,128)(2,1)S(1)} %slice.13.w0), channel_id=1, source_target_pairs={{0,24},{8,0},{16,8},{24,16},{1,25},{9,1},{17,9},{25,17},{2,26},{10... | collective-permute-start | bytes 1179656 | tf_op jit(solution)/shard_map/ppermute | solution.py:378
  191.3 5.1 %collective-permute-done.6.w1 = bf16[16,32,384]{2,1,0:T(8,128)(2,1)S(1)} collective-permute-done((bf16[16,32,384]{2,1,0:T(8,128)(2,1)S(1)}, bf16[16,32,384]{2,1,0:T(8,128)(2,1)S(1)}, u32[]{:S(2)}, u32[]{:S(2)}) %collective-permute-start.6) | collective-permute-done | bytes 393248 | tf_op jit(solution)/shard_map/ppermute | solution.py:378
  196.5 7.8 %collective-permute-done.7.w2 = bf16[16,32,384]{2,1,0:T(8,128)(2,1)S(1)} collective-permute-done((bf16[16,32,384]{2,1,0:T(8,128)(2,1)S(1)}, bf16[16,32,384]{2,1,0:T(8,128)(2,1)S(1)}, u32[]{:S(2)}, u32[]{:S(2)}) %collective-permute-start.7) | collective-permute-done | bytes 393248 | tf_op jit(solution)/shard_map/ppermute | solution.py:378
  206.8 2.9 %shard_map.195 = bf16[4,256,256]{2,1,0:T(8,128)(2,1)S(1)} custom-call(s32[1]{0:T(128)} %bitcast.1.place, s32[1]{0:T(128)} %bitcast.core.place, bf16[4,400,256]{2,1,0:T(8,128)(2,1)S(1)} %all_to_all.31.own, bf16[4,400,256]{2,1,0:T(8,128)(2,1)S(1)} %collective-permute-done.5.other, bf16[16,32,384]{2,1,0:T(8,128)(2,1)S(1)} %slice.13.w0, ...), custom_call_target="tpu_custom_call" | custom-call | tf_op jit(solution)/shard_map/pallas_call | solution.py:347
  209.7 10.8 %all_to_all.32.own = bf16[4,256,256]{2,1,0:T(8,128)(2,1)S(1)} all-to-all(bf16[4,256,256]{2,1,0:T(8,128)(2,1)S(1)} %shard_map.195), channel_id=1, replica_groups=mesh['za'=4,'zb'=2,'zc'=2,'y'=4,'x'=4,'c'=2] {'x'}, dimensions={0} | all-to-all | bytes 1048576 | tf_op jit(solution)/shard_map/all_to_all | solution.py:364
  220.5 3.9 %collective-permute-start.9 = (bf16[4,256,256]{2,1,0:T(8,128)(2,1)S(1)}, bf16[4,256,256]{2,1,0:T(8,128)(2,1)S(1)}, u32[]{:S(2)}, u32[]{:S(2)}) collective-permute-start(bf16[4,256,256]{2,1,0:T(8,128)(2,1)S(1)} %all_to_all.32.own), channel_id=1, source_target_pairs={{0,1},{1,0},{2,3},{3,2},{4,5},{5,4},{6,7},{7,6},{8,9},{9,8},{10,11... | collective-permute-start | bytes 1572872 | tf_op jit(solution)/shard_map/ppermute | solution.py:368
  (67 shorter events, 24.6 us)
Async XLA Ops:
  35.8 4.7 %copy-start.6 = (bf16[128,128]{1,0:T(8,128)(2,1)S(1)}, bf16[128,128]{1,0:T(8,128)(2,1)}, u32[]{:S(2)}) copy-start(bf16[128,128]{1,0:T(8,128)(2,1)} %ls.1) | copy-start | bytes 98308
  35.8 4.7 %copy-start.8 = (f32[2048]{0:T(1024)S(1)}, f32[2048]{0:T(1024)}, u32[]{:S(2)}) copy-start(f32[2048]{0:T(1024)} %param.21) | copy-start | bytes 24580
  35.8 4.7 %copy-start.10 = (f32[128]{0:T(128)S(1)}, f32[128]{0:T(128)}, u32[]{:S(2)}) copy-start(f32[128]{0:T(128)} %param.27) | copy-start | bytes 1540
  35.8 17.9 %all-to-all-start.1 = ((bf16[4,16,32,384]{3,2,1,0:T(8,128)(2,1)}), bf16[4,16,32,384]{3,2,1,0:T(8,128)(2,1)S(1)}, u32[]{:S(2)}, u32[]{:S(2)}) async-start(bf16[4,16,32,384]{3,2,1,0:T(8,128)(2,1)} %broadcast_in_dim.7), calls=%async_computation.1 | async-start | bytes 3145728 | tf_op jit(solution)/shard_map/all_to_all | solution.py:360
  54.7 19.9 %copy-start.16 = (bf16[32,256]{1,0:T(8,128)(2,1)S(1)}, bf16[32,256]{1,0:T(8,128)(2,1)}, u32[]{:S(2)}) copy-start(bf16[32,256]{1,0:T(8,128)(2,1)} %param.39) | copy-start | bytes 49156
  54.8 19.9 %copy-start.19 = (bf16[32,128]{1,0:T(8,128)(2,1)S(1)}, bf16[32,128]{1,0:T(8,128)(2,1)}, u32[]{:S(2)}) copy-start(bf16[32,128]{1,0:T(8,128)(2,1)} %param.38) | copy-start | bytes 24580
  54.8 35.7 %copy-start.17 = (bf16[32,256]{1,0:T(8,128)(2,1)S(1)}, bf16[32,256]{1,0:T(8,128)(2,1)}, u32[]{:S(2)}) copy-start(bf16[32,256]{1,0:T(8,128)(2,1)} %param.26) | copy-start | bytes 49156
  54.8 35.7 %copy-start.18 = (bf16[32,256]{1,0:T(8,128)(2,1)S(1)}, bf16[32,256]{1,0:T(8,128)(2,1)}, u32[]{:S(2)}) copy-start(bf16[32,256]{1,0:T(8,128)(2,1)} %param.25) | copy-start | bytes 49156
  61.2 69.2 %all-to-all-start.2 = ((bf16[16,128,128]{2,1,0:T(8,128)(2,1)}), bf16[16,128,128]{2,1,0:T(8,128)(2,1)S(1)}, u32[]{:S(2)}, u32[]{:S(2)}) async-start(bf16[16,128,128]{2,1,0:T(8,128)(2,1)} %get-tuple-element.13), calls=%async_computation.2 | async-start | bytes 1048576 | tf_op jit(solution)/shard_map/all_to_all | solution.py:364
  74.7 15.7 %collective-permute-start.1 = (bf16[32,384]{1,0:T(8,128)(2,1)S(1)}, bf16[32,384]{1,0:T(8,128)(2,1)S(1)}, u32[]{:S(2)}, u32[]{:S(2)}) collective-permute-start(bf16[32,384]{1,0:T(8,128)(2,1)S(1)} %pad_maximum_fusion.2), channel_id=1, source_target_pairs={{0,0},{1,256},{2,8},{3,264},{4,16},{5,272},{6,24},{7,280},{8,32},{... | collective-permute-start | bytes 73736 | tf_op jit(solution)/shard_map/ppermute | solution.py:416
  90.4 56.0 %copy-start.7 = (f32[31,256]{1,0:T(8,128)S(1)}, f32[31,256]{1,0:T(8,128)}, u32[]{:S(2)}) copy-start(f32[31,256]{1,0:T(8,128)} %taps.1) | copy-start | bytes 95236
  90.4 56.0 %copy-start.9 = (f32[256]{0:T(256)S(1)}, f32[256]{0:T(256)}, u32[]{:S(2)}) copy-start(f32[256]{0:T(256)} %param.37) | copy-start | bytes 3076
  119.9 26.5 %collective-permute-start.2 = (bf16[16,32,512]{2,1,0:T(8,128)(2,1)S(1)}, bf16[16,32,512]{2,1,0:T(8,128)(2,1)S(1)}, u32[]{:S(2)}, u32[]{:S(2)}) collective-permute-start(bf16[16,32,512]{2,1,0:T(8,128)(2,1)S(1)} %slice.12.w0), channel_id=1, source_target_pairs={{0,8},{8,16},{16,24},{24,0},{1,9},{9,17},{17,25},{25,1},{2,10},{10... | collective-permute-start | bytes 1572872 | tf_op jit(solution)/shard_map/ppermute | solution.py:378
  123.2 23.3 %collective-permute-start.3 = (bf16[16,32,512]{2,1,0:T(8,128)(2,1)S(1)}, bf16[16,32,512]{2,1,0:T(8,128)(2,1)S(1)}, u32[]{:S(2)}, u32[]{:S(2)}) collective-permute-start(bf16[16,32,512]{2,1,0:T(8,128)(2,1)S(1)} %slice.12.w0), channel_id=1, source_target_pairs={{0,16},{8,24},{16,0},{24,8},{1,17},{9,25},{17,1},{25,9},{2,18},{10... | collective-permute-start | bytes 1572872 | tf_op jit(solution)/shard_map/ppermute | solution.py:378
  127.7 18.7 %collective-permute-start.4 = (bf16[16,32,512]{2,1,0:T(8,128)(2,1)S(1)}, bf16[16,32,512]{2,1,0:T(8,128)(2,1)}, u32[]{:S(2)}, u32[]{:S(2)}) collective-permute-start(bf16[16,32,512]{2,1,0:T(8,128)(2,1)S(1)} %slice.12.w0), channel_id=1, source_target_pairs={{0,24},{8,0},{16,8},{24,16},{1,25},{9,1},{17,9},{25,17},{2,26},{10... | collective-permute-start | bytes 1572872 | tf_op jit(solution)/shard_map/ppermute | solution.py:378
  132.6 19.3 %all-to-all-start.3 = ((bf16[4,128,128]{2,1,0:T(8,128)(2,1)}), bf16[4,128,128]{2,1,0:T(8,128)(2,1)S(1)}, u32[]{:S(2)}, u32[]{:S(2)}) async-start(bf16[4,128,128]{2,1,0:T(8,128)(2,1)} %get-tuple-element.14), calls=%async_computation.3 | async-start | bytes 262144 | tf_op jit(solution)/shard_map/all_to_all | solution.py:364
  140.4 6.0 %collective-permute-start = (bf16[32,2048]{1,0:T(8,128)(2,1)S(1)}, bf16[32,2048]{1,0:T(8,128)(2,1)S(1)}, u32[]{:S(2)}, u32[]{:S(2)}) collective-permute-start(bf16[32,2048]{1,0:T(8,128)(2,1)S(1)} %slice.9), channel_id=1, source_target_pairs={{0,8},{8,16},{16,24},{24,32},{32,40},{40,48},{48,56},{56,64},{64,7... | collective-permute-start | bytes 393224 | tf_op jit(solution)/shard_map/ppermute | solution.py:409
  146.5 5.4 %copy-start.12 = (f32[128]{0:T(128)S(1)}, f32[128]{0:T(128)}, u32[]{:S(2)}) copy-start(f32[128]{0:T(128)} %param.35) | copy-start | bytes 1540
  167.9 38.9 %collective-permute-start.5 = (bf16[4,400,256]{2,1,0:T(8,128)(2,1)S(1)}, bf16[4,400,256]{2,1,0:T(8,128)(2,1)S(1)}, u32[]{:S(2)}, u32[]{:S(2)}) collective-permute-start(bf16[4,400,256]{2,1,0:T(8,128)(2,1)S(1)} %all_to_all.31.own), channel_id=1, source_target_pairs={{0,1},{1,0},{2,3},{3,2},{4,5},{5,4},{6,7},{7,6},{8,9},{9,8},{10,11... | collective-permute-start | bytes 2457608 | tf_op jit(solution)/shard_map/ppermute | solution.py:368
  182.3 14.1 %collective-permute-start.6 = (bf16[16,32,384]{2,1,0:T(8,128)(2,1)S(1)}, bf16[16,32,384]{2,1,0:T(8,128)(2,1)S(1)}, u32[]{:S(2)}, u32[]{:S(2)}) collective-permute-start(bf16[16,32,384]{2,1,0:T(8,128)(2,1)S(1)} %slice.13.w0), channel_id=1, source_target_pairs={{0,8},{8,16},{16,24},{24,0},{1,9},{9,17},{17,25},{25,1},{2,10},{10... | collective-permute-start | bytes 1179656 | tf_op jit(solution)/shard_map/ppermute | solution.py:378
  184.3 19.9 %collective-permute-start.7 = (bf16[16,32,384]{2,1,0:T(8,128)(2,1)S(1)}, bf16[16,32,384]{2,1,0:T(8,128)(2,1)S(1)}, u32[]{:S(2)}, u32[]{:S(2)}) collective-permute-start(bf16[16,32,384]{2,1,0:T(8,128)(2,1)S(1)} %slice.13.w0), channel_id=1, source_target_pairs={{0,16},{8,24},{16,0},{24,8},{1,17},{9,25},{17,1},{25,9},{2,18},{10... | collective-permute-start | bytes 1179656 | tf_op jit(solution)/shard_map/ppermute | solution.py:378
  188.5 18.3 %collective-permute-start.8 = (bf16[16,32,384]{2,1,0:T(8,128)(2,1)S(1)}, bf16[16,32,384]{2,1,0:T(8,128)(2,1)S(1)}, u32[]{:S(2)}, u32[]{:S(2)}) collective-permute-start(bf16[16,32,384]{2,1,0:T(8,128)(2,1)S(1)} %slice.13.w0), channel_id=1, source_target_pairs={{0,24},{8,0},{16,8},{24,16},{1,25},{9,1},{17,9},{25,17},{2,26},{10... | collective-permute-start | bytes 1179656 | tf_op jit(solution)/shard_map/ppermute | solution.py:378
  220.5 5.4 %copy-start.14 = (bf16[4,256,256]{2,1,0:T(8,128)(2,1)}, bf16[4,256,256]{2,1,0:T(8,128)(2,1)S(1)}, u32[]{:S(2)}) copy-start(bf16[4,256,256]{2,1,0:T(8,128)(2,1)S(1)} %all_to_all.32.own) | copy-start | bytes 1572868
  220.5 5.4 %collective-permute-start.9 = (bf16[4,256,256]{2,1,0:T(8,128)(2,1)S(1)}, bf16[4,256,256]{2,1,0:T(8,128)(2,1)S(1)}, u32[]{:S(2)}, u32[]{:S(2)}) collective-permute-start(bf16[4,256,256]{2,1,0:T(8,128)(2,1)S(1)} %all_to_all.32.own), channel_id=1, source_target_pairs={{0,1},{1,0},{2,3},{3,2},{4,5},{5,4},{6,7},{7,6},{8,9},{9,8},{10,11... | collective-permute-start | bytes 1572872 | tf_op jit(solution)/shard_map/ppermute | solution.py:368
  (11 other events, 28.7 us)

commit v4 on v3

--- a/solution.py
+++ b/solution.py
@@ -324,19 +324,28 @@
         out[k] = total
 
 
-def place_kernel(place, own, other, out, sems):
-    c = place[0]
+def fan_kernel(x, out):
+    for k in range(4):
+        out[k] = x[...]
+
+
+def place_blocks(core, blocks, out, sems):
     copies = []
     for x in range(4):
-        for k, (src, core) in enumerate(((own, c), (other, 1 - c))):
-            at = pl.multiple_of((2 * x + core) * 256, 256)
-            copies.append(
-                pltpu.make_async_copy(src.at[x], out.at[:, pl.ds(at, 256)], sems.at[2 * x + k])
-            )
+        at = pl.multiple_of((2 * x + core) * 256, 256)
+        copies.append(pltpu.make_async_copy(blocks.at[x], out.at[:, pl.ds(at, 256)], sems.at[x]))
     for copy in copies:
         copy.start()
     for copy in copies:
         copy.wait()
+
+
+def place_own(place, own, out, sems):
+    place_blocks(place[0], own, out, sems)
+
+
+def place_other(place, other, begun, out, sems):
+    place_blocks(1 - place[0], other, out, sems)
 
 
 VM = pl.BlockSpec(memory_space=pltpu.VMEM)
@@ -405,7 +414,9 @@
     gain = row(input_norm_gain)
     w_state = jnp.concatenate([query_matrix, key_matrix, value_matrix], axis=1)
     w_out = jnp.concatenate([attention_output_matrix, convolution_output_matrix], axis=1)
-    w_state = everyone(everyone(w_state, Z), "y")
+    w_state = everyone(w_state, Z)
+    (w_state,) = call(fan_kernel, [((4, 16, 32, 384), BF)], (w_state,))
+    w_state = exchange(w_state, "y")
     halo = lax.ppermute(tokens[TOK - HALO :], SP, [(i, i + 1) for i in range(63)])
     moves = []
     for a in range(8):
@@ -474,14 +485,24 @@
     own = exchange(out, "x")
     other = other_core(own)
     hbm = pl.BlockSpec(memory_space=pl.ANY)
+    c = placed("c")
+    whole = pl.pallas_call(
+        place_own,
+        out_shape=jax.ShapeDtypeStruct((TOK, DIM), BF),
+        in_specs=[SM, VM],
+        out_specs=hbm,
+        scratch_shapes=[pltpu.SemaphoreType.DMA((4,))],
+        name="begin",
+    )(c, own)
     return pl.pallas_call(
-        place_kernel,
+        place_other,
         out_shape=jax.ShapeDtypeStruct((TOK, DIM), BF),
-        in_specs=[SM, VM, VM],
+        in_specs=[SM, VM, hbm],
         out_specs=hbm,
-        scratch_shapes=[pltpu.SemaphoreType.DMA((8,))],
+        scratch_shapes=[pltpu.SemaphoreType.DMA((4,))],
+        input_output_aliases={2: 0},
         name="place",
-    )(placed("c"), own, other)
+    )(c, other, whole)
 
 
 def solution(mesh):

time: 230 us -> 230 us (level)
  Pallas kernels: 20.1 us -> 22.8 us
    all_to_all x2 -> x3, waiting for transfers between devices: 1.51 us -> 10.3 us  [exchange(): return lax.all_to_all(copies, axis, split_axis=0, concat_axis=0, tiled=True)]
    all_to_all x1 -> x0, waiting for transfers between devices: 8.67 us -> none  [everyone(): return lax.all_to_all(copies, axis, split_axis=0, concat_axis=0, tiled=True)]
    all_to_all x2 -> x3, starting transfers between devices: 20.3 us -> 24.6 us  [exchange(): return lax.all_to_all(copies, axis, split_axis=0, concat_axis=0, tiled=True)]
    all_to_all x1 -> x0, starting transfers between devices: 4.33 us -> none  [everyone(): return lax.all_to_all(copies, axis, split_axis=0, concat_axis=0, tiled=True)]
    pallas_call x6 -> x7, Pallas kernels: 17.9 us -> 19 us  [call(): pl.pallas_call(kernel, out_shape=[jax.ShapeDtypeStruct(s, d) for s, d in...]
  transfers between devices with their start and end apart: 13 -> 13, of which waited for: 8 -> 7; matrix products, arithmetic and copies ran while one was open for 1% -> 1% of each run, Pallas kernels for 3% -> 4%
where the time goes in v4:
time: 230 us; the launch traced here: 229 us
  blocking collectives  88.1 us (38%)
  starting transfers between devices  75.2 us (33%)
  waiting for transfers between devices  33.6 us (15%)
  Pallas kernels  22.8 us (10%)
  local copies, waits for them, and re-layouts  8.09 us (4%)
    all_to_all x1, blocking collectives, everyone(): return lax.all_to_all(copies, axis, split_axis=0, concat_axis=0, tiled=True)  33.6 us
    all_gather x1, blocking collectives, layer(): rest = lax.all_gather(rest, Z)  28.5 us
    all_to_all x2, blocking collectives, exchange(): return lax.all_to_all(copies, axis, split_axis=0, concat_axis=0, tiled=True)  25.9 us
    all_to_all x3, starting transfers between devices, exchange(): return lax.all_to_all(copies, axis, split_axis=0, concat_axis=0, tiled=True)  24.6 us
    ppermute x6, starting transfers between devices, neighbours(): pieces.append(lax.ppermute(x, 'y', [(i, (i + k) % 4) for i in range(4)]))  19.4 us
    pallas_call x7, Pallas kernels, call(): pl.pallas_call(kernel, out_shape=[jax.ShapeDtypeStruct(s, d) for s, d in...  19 us
    ppermute x2, starting transfers between devices, other_core(): return lax.ppermute(x, 'c', [(0, 1), (1, 0)])  17.3 us
    ppermute x6, waiting for transfers between devices, neighbours(): pieces.append(lax.ppermute(x, 'y', [(i, (i + k) % 4) for i in range(4)]))  15.4 us
  transfers between devices with their start and end apart: 13, of which 7 were waited for; matrix products, arithmetic and copies ran while one was open for 1% of the time, Pallas kernels for 4%

profile of v4, /device:TPU:1, one launch (start us, length us, event | category | flops | bytes accessed | tf_op | source)
XLA Modules:
  0.0 229.0 jit_solution(14932182973891937560)
XLA Ops:
  0.8 33.6 %all_to_all.30.x = bf16[16,32,384]{2,1,0:T(8,128)(2,1)S(1)} all-to-all(bf16[16,32,384]{2,1,0:T(8,128)(2,1)S(1)} %broadcast_in_dim.3), channel_id=1, replica_groups=mesh['za'=4,'zb'=2,'zc'=2,'y'=4,'x'=4,'c'=2] {'za','zb','zc'}, dimensions={0} | all-to-all | bytes 786432 | tf_op jit(solution)/shard_map/all_to_all | solution.py:369
  35.8 4.3 %all-to-all-start.1 = ((bf16[4,16,32,384]{3,2,1,0:T(8,128)(2,1)}), bf16[4,16,32,384]{3,2,1,0:T(8,128)(2,1)S(1)}, u32[]{:S(2)}, u32[]{:S(2)}) async-start(bf16[4,16,32,384]{3,2,1,0:T(8,128)(2,1)} %shard_map.191), calls=%async_computation.1 | async-start | bytes 3145728 | tf_op jit(solution)/shard_map/all_to_all | solution.py:373
  45.0 8.7 %all-to-all-done.1.w = bf16[4,16,32,384]{3,2,1,0:T(8,128)(2,1)S(1)} async-done(((bf16[4,16,32,384]{3,2,1,0:T(8,128)(2,1)}), bf16[4,16,32,384]{3,2,1,0:T(8,128)(2,1)S(1)}, u32[]{:S(2)}, u32[]{:S(2)}) %all-to-all-start.1) | async-done | bytes 1572896 | tf_op jit(solution)/shard_map/all_to_all | solution.py:373
  54.7 6.4 %shard_map.192 = (f32[2,256,128]{2,1,0:T(8,128)S(1)}, bf16[16,128,128]{2,1,0:T(8,128)(2,1)}) custom-call(bf16[256,2048]{1,0:T(8,128)(2,1)S(1)} %get-tuple-element.11.x, bf16[4,16,32,384]{3,2,1,0:T(8,128)(2,1)S(1)} %all-to-all-done.1.w, f32[3,256,128]{2,1,0:T(8,128)S(1)} %copy-done.4), custom_call_target="tpu_custom_call" | custom-call | tf_op jit(solution)/shard_map/pallas_call | solution.py:356
  61.2 13.4 %all-to-all-start.2 = ((bf16[16,128,128]{2,1,0:T(8,128)(2,1)}), bf16[16,128,128]{2,1,0:T(8,128)(2,1)S(1)}, u32[]{:S(2)}, u32[]{:S(2)}) async-start(bf16[16,128,128]{2,1,0:T(8,128)(2,1)} %get-tuple-element.13), calls=%async_computation.2 | async-start | bytes 1048576 | tf_op jit(solution)/shard_map/all_to_all | solution.py:373
  74.6 10.9 %collective-permute-start.1 = (bf16[32,384]{1,0:T(8,128)(2,1)S(1)}, bf16[32,384]{1,0:T(8,128)(2,1)S(1)}, u32[]{:S(2)}, u32[]{:S(2)}) collective-permute-start(bf16[32,384]{1,0:T(8,128)(2,1)S(1)} %pad_maximum_fusion.2), channel_id=1, source_target_pairs={{0,0},{1,256},{2,8},{3,264},{4,16},{5,272},{6,24},{7,280},{8,32},{... | collective-permute-start | bytes 73736 | tf_op jit(solution)/shard_map/ppermute | solution.py:427
  85.6 4.8 %collective-permute-done.1 = bf16[32,384]{1,0:T(8,128)(2,1)S(1)} collective-permute-done((bf16[32,384]{1,0:T(8,128)(2,1)S(1)}, bf16[32,384]{1,0:T(8,128)(2,1)S(1)}, u32[]{:S(2)}, u32[]{:S(2)}) %collective-permute-start.1) | collective-permute-done | bytes 24608 | tf_op jit(solution)/shard_map/ppermute | solution.py:427
  90.4 28.5 %all-gather = bf16[512,896]{1,0:T(8,128)(2,1)S(1)} all-gather(bf16[32,896]{1,0:T(8,128)(2,1)S(1)} %pad_maximum_fusion), channel_id=2, replica_groups=mesh['za'=4,'zb'=2,'zc'=2,'y'=4,'x'=4,'c'=2] {'za','zb','zc'}, dimensions={0}, use_global_device_ids=true | all-gather | bytes 974848 | tf_op jit(solution)/shard_map/all_gather | solution.py:429
  119.9 3.2 %collective-permute-start.2 = (bf16[16,32,512]{2,1,0:T(8,128)(2,1)S(1)}, bf16[16,32,512]{2,1,0:T(8,128)(2,1)S(1)}, u32[]{:S(2)}, u32[]{:S(2)}) collective-permute-start(bf16[16,32,512]{2,1,0:T(8,128)(2,1)S(1)} %slice.12.w0), channel_id=1, source_target_pairs={{0,8},{8,16},{16,24},{24,0},{1,9},{9,17},{17,25},{25,1},{2,10},{10... | collective-permute-start | bytes 1572872 | tf_op jit(solution)/shard_map/ppermute | solution.py:387
  123.1 4.5 %collective-permute-start.3 = (bf16[16,32,512]{2,1,0:T(8,128)(2,1)S(1)}, bf16[16,32,512]{2,1,0:T(8,128)(2,1)S(1)}, u32[]{:S(2)}, u32[]{:S(2)}) collective-permute-start(bf16[16,32,512]{2,1,0:T(8,128)(2,1)S(1)} %slice.12.w0), channel_id=1, source_target_pairs={{0,16},{8,24},{16,0},{24,8},{1,17},{9,25},{17,1},{25,9},{2,18},{10... | collective-permute-start | bytes 1572872 | tf_op jit(solution)/shard_map/ppermute | solution.py:387
  127.7 2.7 %collective-permute-start.4 = (bf16[16,32,512]{2,1,0:T(8,128)(2,1)S(1)}, bf16[16,32,512]{2,1,0:T(8,128)(2,1)}, u32[]{:S(2)}, u32[]{:S(2)}) collective-permute-start(bf16[16,32,512]{2,1,0:T(8,128)(2,1)S(1)} %slice.12.w0), channel_id=1, source_target_pairs={{0,24},{8,0},{16,8},{24,16},{1,25},{9,1},{17,9},{25,17},{2,26},{10... | collective-permute-start | bytes 1572872 | tf_op jit(solution)/shard_map/ppermute | solution.py:387
  132.5 6.9 %all-to-all-start.3 = ((bf16[4,128,128]{2,1,0:T(8,128)(2,1)}), bf16[4,128,128]{2,1,0:T(8,128)(2,1)S(1)}, u32[]{:S(2)}, u32[]{:S(2)}) async-start(bf16[4,128,128]{2,1,0:T(8,128)(2,1)} %get-tuple-element.14), calls=%async_computation.3 | async-start | bytes 262144 | tf_op jit(solution)/shard_map/all_to_all | solution.py:373
  140.4 2.9 %collective-permute-start = (bf16[32,2048]{1,0:T(8,128)(2,1)S(1)}, bf16[32,2048]{1,0:T(8,128)(2,1)S(1)}, u32[]{:S(2)}, u32[]{:S(2)}) collective-permute-start(bf16[32,2048]{1,0:T(8,128)(2,1)S(1)} %slice.9), channel_id=1, source_target_pairs={{0,8},{8,16},{16,24},{24,32},{32,40},{40,48},{48,56},{56,64},{64,7... | collective-permute-start | bytes 393224 | tf_op jit(solution)/shard_map/ppermute | solution.py:420
  143.3 3.1 %collective-permute-done.halo = bf16[32,2048]{1,0:T(8,128)(2,1)S(1)} collective-permute-done((bf16[32,2048]{1,0:T(8,128)(2,1)S(1)}, bf16[32,2048]{1,0:T(8,128)(2,1)S(1)}, u32[]{:S(2)}, u32[]{:S(2)}) %collective-permute-start) | collective-permute-done | bytes 131104 | tf_op jit(solution)/shard_map/ppermute | solution.py:420
  146.4 3.8 %shard_map.194.dev = bf16[272,256]{1,0:T(8,128)(2,1)S(1)} custom-call(s32[1]{0:T(128)} %bitcast.1.place, bf16[256,2048]{1,0:T(8,128)(2,1)S(1)} %get-tuple-element.11.x, bf16[32,2048]{1,0:T(8,128)(2,1)S(1)} %collective-permute-done.halo, f32[1,2048]{1,0:T(1,128)S(1)} %bitcast.11, bf16[16,32,512]{2,1,0:T(8,128)(2,1)S(1)} %slice.12.w0, ...), custom_call_target="tpu_custom_call" | custom-call | tf_op jit(solution)/shard_map/pallas_call | solution.py:356
  152.8 15.1 %all_to_all.31.own = bf16[4,400,256]{2,1,0:T(8,128)(2,1)S(1)} all-to-all(bf16[4,400,256]{2,1,0:T(8,128)(2,1)S(1)} %shard_map.195), channel_id=1, replica_groups=mesh['za'=4,'zb'=2,'zc'=2,'y'=4,'x'=4,'c'=2] {'x'}, dimensions={0} | all-to-all | bytes 1638400 | tf_op jit(solution)/shard_map/all_to_all | solution.py:373
  167.9 13.3 %collective-permute-start.5 = (bf16[4,400,256]{2,1,0:T(8,128)(2,1)S(1)}, bf16[4,400,256]{2,1,0:T(8,128)(2,1)S(1)}, u32[]{:S(2)}, u32[]{:S(2)}) collective-permute-start(bf16[4,400,256]{2,1,0:T(8,128)(2,1)S(1)} %all_to_all.31.own), channel_id=1, source_target_pairs={{0,1},{1,0},{2,3},{3,2},{4,5},{5,4},{6,7},{7,6},{8,9},{9,8},{10,11... | collective-permute-start | bytes 2457608 | tf_op jit(solution)/shard_map/ppermute | solution.py:377
  184.2 4.2 %collective-permute-start.7 = (bf16[16,32,384]{2,1,0:T(8,128)(2,1)S(1)}, bf16[16,32,384]{2,1,0:T(8,128)(2,1)S(1)}, u32[]{:S(2)}, u32[]{:S(2)}) collective-permute-start(bf16[16,32,384]{2,1,0:T(8,128)(2,1)S(1)} %slice.13.w0), channel_id=1, source_target_pairs={{0,16},{8,24},{16,0},{24,8},{1,17},{9,25},{17,1},{25,9},{2,18},{10... | collective-permute-start | bytes 1179656 | tf_op jit(solution)/shard_map/ppermute | solution.py:387
  188.4 2.9 %collective-permute-start.8 = (bf16[16,32,384]{2,1,0:T(8,128)(2,1)S(1)}, bf16[16,32,384]{2,1,0:T(8,128)(2,1)S(1)}, u32[]{:S(2)}, u32[]{:S(2)}) collective-permute-start(bf16[16,32,384]{2,1,0:T(8,128)(2,1)S(1)} %slice.13.w0), channel_id=1, source_target_pairs={{0,24},{8,0},{16,8},{24,16},{1,25},{9,1},{17,9},{25,17},{2,26},{10... | collective-permute-start | bytes 1179656 | tf_op jit(solution)/shard_map/ppermute | solution.py:387
  191.3 5.1 %collective-permute-done.6.w1 = bf16[16,32,384]{2,1,0:T(8,128)(2,1)S(1)} collective-permute-done((bf16[16,32,384]{2,1,0:T(8,128)(2,1)S(1)}, bf16[16,32,384]{2,1,0:T(8,128)(2,1)S(1)}, u32[]{:S(2)}, u32[]{:S(2)}) %collective-permute-start.6) | collective-permute-done | bytes 393248 | tf_op jit(solution)/shard_map/ppermute | solution.py:387
  196.4 7.8 %collective-permute-done.7.w2 = bf16[16,32,384]{2,1,0:T(8,128)(2,1)S(1)} collective-permute-done((bf16[16,32,384]{2,1,0:T(8,128)(2,1)S(1)}, bf16[16,32,384]{2,1,0:T(8,128)(2,1)S(1)}, u32[]{:S(2)}, u32[]{:S(2)}) %collective-permute-start.7) | collective-permute-done | bytes 393248 | tf_op jit(solution)/shard_map/ppermute | solution.py:387
  206.7 2.9 %shard_map.196 = bf16[4,256,256]{2,1,0:T(8,128)(2,1)S(1)} custom-call(s32[1]{0:T(128)} %bitcast.1.place, s32[1]{0:T(128)} %bitcast.core.place, bf16[4,400,256]{2,1,0:T(8,128)(2,1)S(1)} %all_to_all.31.own, bf16[4,400,256]{2,1,0:T(8,128)(2,1)S(1)} %collective-permute-done.5.other, bf16[16,32,384]{2,1,0:T(8,128)(2,1)S(1)} %slice.13.w0, ...), custom_call_target="tpu_custom_call" | custom-call | tf_op jit(solution)/shard_map/pallas_call | solution.py:356
  209.6 10.8 %all_to_all.32.own = bf16[4,256,256]{2,1,0:T(8,128)(2,1)S(1)} all-to-all(bf16[4,256,256]{2,1,0:T(8,128)(2,1)S(1)} %shard_map.196), channel_id=1, replica_groups=mesh['za'=4,'zb'=2,'zc'=2,'y'=4,'x'=4,'c'=2] {'x'}, dimensions={0} | all-to-all | bytes 1048576 | tf_op jit(solution)/shard_map/all_to_all | solution.py:373
  220.4 3.9 %collective-permute-start.9 = (bf16[4,256,256]{2,1,0:T(8,128)(2,1)S(1)}, bf16[4,256,256]{2,1,0:T(8,128)(2,1)S(1)}, u32[]{:S(2)}, u32[]{:S(2)}) collective-permute-start(bf16[4,256,256]{2,1,0:T(8,128)(2,1)S(1)} %all_to_all.32.own), channel_id=1, source_target_pairs={{0,1},{1,0},{2,3},{3,2},{4,5},{5,4},{6,7},{7,6},{8,9},{9,8},{10,11... | collective-permute-start | bytes 1572872 | tf_op jit(solution)/shard_map/ppermute | solution.py:377
  (68 shorter events, 24.6 us)
Async XLA Ops:
  35.7 4.7 %copy-start.5 = (bf16[128,128]{1,0:T(8,128)(2,1)S(1)}, bf16[128,128]{1,0:T(8,128)(2,1)}, u32[]{:S(2)}) copy-start(bf16[128,128]{1,0:T(8,128)(2,1)} %ds.1) | copy-start | bytes 98308
  35.8 4.7 %copy-start.6 = (bf16[128,128]{1,0:T(8,128)(2,1)S(1)}, bf16[128,128]{1,0:T(8,128)(2,1)}, u32[]{:S(2)}) copy-start(bf16[128,128]{1,0:T(8,128)(2,1)} %ls.1) | copy-start | bytes 98308
  35.8 4.7 %copy-start.8 = (f32[2048]{0:T(1024)S(1)}, f32[2048]{0:T(1024)}, u32[]{:S(2)}) copy-start(f32[2048]{0:T(1024)} %param.21) | copy-start | bytes 24580
  35.8 4.7 %copy-start.10 = (f32[128]{0:T(128)S(1)}, f32[128]{0:T(128)}, u32[]{:S(2)}) copy-start(f32[128]{0:T(128)} %param.27) | copy-start | bytes 1540
  35.8 17.9 %all-to-all-start.1 = ((bf16[4,16,32,384]{3,2,1,0:T(8,128)(2,1)}), bf16[4,16,32,384]{3,2,1,0:T(8,128)(2,1)S(1)}, u32[]{:S(2)}, u32[]{:S(2)}) async-start(bf16[4,16,32,384]{3,2,1,0:T(8,128)(2,1)} %shard_map.191), calls=%async_computation.1 | async-start | bytes 3145728 | tf_op jit(solution)/shard_map/all_to_all | solution.py:373
  54.7 19.9 %copy-start.16 = (bf16[32,256]{1,0:T(8,128)(2,1)S(1)}, bf16[32,256]{1,0:T(8,128)(2,1)}, u32[]{:S(2)}) copy-start(bf16[32,256]{1,0:T(8,128)(2,1)} %param.39) | copy-start | bytes 49156
  54.7 19.9 %copy-start.19 = (bf16[32,128]{1,0:T(8,128)(2,1)S(1)}, bf16[32,128]{1,0:T(8,128)(2,1)}, u32[]{:S(2)}) copy-start(bf16[32,128]{1,0:T(8,128)(2,1)} %param.38) | copy-start | bytes 24580
  54.7 35.6 %copy-start.17 = (bf16[32,256]{1,0:T(8,128)(2,1)S(1)}, bf16[32,256]{1,0:T(8,128)(2,1)}, u32[]{:S(2)}) copy-start(bf16[32,256]{1,0:T(8,128)(2,1)} %param.26) | copy-start | bytes 49156
  54.7 35.6 %copy-start.18 = (bf16[32,256]{1,0:T(8,128)(2,1)S(1)}, bf16[32,256]{1,0:T(8,128)(2,1)}, u32[]{:S(2)}) copy-start(bf16[32,256]{1,0:T(8,128)(2,1)} %param.25) | copy-start | bytes 49156
  61.2 69.2 %all-to-all-start.2 = ((bf16[16,128,128]{2,1,0:T(8,128)(2,1)}), bf16[16,128,128]{2,1,0:T(8,128)(2,1)S(1)}, u32[]{:S(2)}, u32[]{:S(2)}) async-start(bf16[16,128,128]{2,1,0:T(8,128)(2,1)} %get-tuple-element.13), calls=%async_computation.2 | async-start | bytes 1048576 | tf_op jit(solution)/shard_map/all_to_all | solution.py:373
  74.6 15.7 %collective-permute-start.1 = (bf16[32,384]{1,0:T(8,128)(2,1)S(1)}, bf16[32,384]{1,0:T(8,128)(2,1)S(1)}, u32[]{:S(2)}, u32[]{:S(2)}) collective-permute-start(bf16[32,384]{1,0:T(8,128)(2,1)S(1)} %pad_maximum_fusion.2), channel_id=1, source_target_pairs={{0,0},{1,256},{2,8},{3,264},{4,16},{5,272},{6,24},{7,280},{8,32},{... | collective-permute-start | bytes 73736 | tf_op jit(solution)/shard_map/ppermute | solution.py:427
  90.4 56.0 %copy-start.7 = (f32[31,256]{1,0:T(8,128)S(1)}, f32[31,256]{1,0:T(8,128)}, u32[]{:S(2)}) copy-start(f32[31,256]{1,0:T(8,128)} %taps.1) | copy-start | bytes 95236
  90.4 56.0 %copy-start.9 = (f32[256]{0:T(256)S(1)}, f32[256]{0:T(256)}, u32[]{:S(2)}) copy-start(f32[256]{0:T(256)} %param.37) | copy-start | bytes 3076
  119.9 26.5 %collective-permute-start.2 = (bf16[16,32,512]{2,1,0:T(8,128)(2,1)S(1)}, bf16[16,32,512]{2,1,0:T(8,128)(2,1)S(1)}, u32[]{:S(2)}, u32[]{:S(2)}) collective-permute-start(bf16[16,32,512]{2,1,0:T(8,128)(2,1)S(1)} %slice.12.w0), channel_id=1, source_target_pairs={{0,8},{8,16},{16,24},{24,0},{1,9},{9,17},{17,25},{25,1},{2,10},{10... | collective-permute-start | bytes 1572872 | tf_op jit(solution)/shard_map/ppermute | solution.py:387
  123.1 23.3 %collective-permute-start.3 = (bf16[16,32,512]{2,1,0:T(8,128)(2,1)S(1)}, bf16[16,32,512]{2,1,0:T(8,128)(2,1)S(1)}, u32[]{:S(2)}, u32[]{:S(2)}) collective-permute-start(bf16[16,32,512]{2,1,0:T(8,128)(2,1)S(1)} %slice.12.w0), channel_id=1, source_target_pairs={{0,16},{8,24},{16,0},{24,8},{1,17},{9,25},{17,1},{25,9},{2,18},{10... | collective-permute-start | bytes 1572872 | tf_op jit(solution)/shard_map/ppermute | solution.py:387
  127.7 18.7 %collective-permute-start.4 = (bf16[16,32,512]{2,1,0:T(8,128)(2,1)S(1)}, bf16[16,32,512]{2,1,0:T(8,128)(2,1)}, u32[]{:S(2)}, u32[]{:S(2)}) collective-permute-start(bf16[16,32,512]{2,1,0:T(8,128)(2,1)S(1)} %slice.12.w0), channel_id=1, source_target_pairs={{0,24},{8,0},{16,8},{24,16},{1,25},{9,1},{17,9},{25,17},{2,26},{10... | collective-permute-start | bytes 1572872 | tf_op jit(solution)/shard_map/ppermute | solution.py:387
  132.5 19.3 %all-to-all-start.3 = ((bf16[4,128,128]{2,1,0:T(8,128)(2,1)}), bf16[4,128,128]{2,1,0:T(8,128)(2,1)S(1)}, u32[]{:S(2)}, u32[]{:S(2)}) async-start(bf16[4,128,128]{2,1,0:T(8,128)(2,1)} %get-tuple-element.14), calls=%async_computation.3 | async-start | bytes 262144 | tf_op jit(solution)/shard_map/all_to_all | solution.py:373
  140.4 6.0 %collective-permute-start = (bf16[32,2048]{1,0:T(8,128)(2,1)S(1)}, bf16[32,2048]{1,0:T(8,128)(2,1)S(1)}, u32[]{:S(2)}, u32[]{:S(2)}) collective-permute-start(bf16[32,2048]{1,0:T(8,128)(2,1)S(1)} %slice.9), channel_id=1, source_target_pairs={{0,8},{8,16},{16,24},{24,32},{32,40},{40,48},{48,56},{56,64},{64,7... | collective-permute-start | bytes 393224 | tf_op jit(solution)/shard_map/ppermute | solution.py:420
  146.4 5.4 %copy-start.12 = (f32[128]{0:T(128)S(1)}, f32[128]{0:T(128)}, u32[]{:S(2)}) copy-start(f32[128]{0:T(128)} %param.35) | copy-start | bytes 1540
  167.9 38.8 %collective-permute-start.5 = (bf16[4,400,256]{2,1,0:T(8,128)(2,1)S(1)}, bf16[4,400,256]{2,1,0:T(8,128)(2,1)S(1)}, u32[]{:S(2)}, u32[]{:S(2)}) collective-permute-start(bf16[4,400,256]{2,1,0:T(8,128)(2,1)S(1)} %all_to_all.31.own), channel_id=1, source_target_pairs={{0,1},{1,0},{2,3},{3,2},{4,5},{5,4},{6,7},{7,6},{8,9},{9,8},{10,11... | collective-permute-start | bytes 2457608 | tf_op jit(solution)/shard_map/ppermute | solution.py:377
  182.3 14.1 %collective-permute-start.6 = (bf16[16,32,384]{2,1,0:T(8,128)(2,1)S(1)}, bf16[16,32,384]{2,1,0:T(8,128)(2,1)S(1)}, u32[]{:S(2)}, u32[]{:S(2)}) collective-permute-start(bf16[16,32,384]{2,1,0:T(8,128)(2,1)S(1)} %slice.13.w0), channel_id=1, source_target_pairs={{0,8},{8,16},{16,24},{24,0},{1,9},{9,17},{17,25},{25,1},{2,10},{10... | collective-permute-start | bytes 1179656 | tf_op jit(solution)/shard_map/ppermute | solution.py:387
  184.2 19.9 %collective-permute-start.7 = (bf16[16,32,384]{2,1,0:T(8,128)(2,1)S(1)}, bf16[16,32,384]{2,1,0:T(8,128)(2,1)S(1)}, u32[]{:S(2)}, u32[]{:S(2)}) collective-permute-start(bf16[16,32,384]{2,1,0:T(8,128)(2,1)S(1)} %slice.13.w0), channel_id=1, source_target_pairs={{0,16},{8,24},{16,0},{24,8},{1,17},{9,25},{17,1},{25,9},{2,18},{10... | collective-permute-start | bytes 1179656 | tf_op jit(solution)/shard_map/ppermute | solution.py:387
  188.4 18.3 %collective-permute-start.8 = (bf16[16,32,384]{2,1,0:T(8,128)(2,1)S(1)}, bf16[16,32,384]{2,1,0:T(8,128)(2,1)S(1)}, u32[]{:S(2)}, u32[]{:S(2)}) collective-permute-start(bf16[16,32,384]{2,1,0:T(8,128)(2,1)S(1)} %slice.13.w0), channel_id=1, source_target_pairs={{0,24},{8,0},{16,8},{24,16},{1,25},{9,1},{17,9},{25,17},{2,26},{10... | collective-permute-start | bytes 1179656 | tf_op jit(solution)/shard_map/ppermute | solution.py:387
  220.4 5.8 %collective-permute-start.9 = (bf16[4,256,256]{2,1,0:T(8,128)(2,1)S(1)}, bf16[4,256,256]{2,1,0:T(8,128)(2,1)S(1)}, u32[]{:S(2)}, u32[]{:S(2)}) collective-permute-start(bf16[4,256,256]{2,1,0:T(8,128)(2,1)S(1)} %all_to_all.32.own), channel_id=1, source_target_pairs={{0,1},{1,0},{2,3},{3,2},{4,5},{5,4},{6,7},{7,6},{8,9},{9,8},{10,11... | collective-permute-start | bytes 1572872 | tf_op jit(solution)/shard_map/ppermute | solution.py:377
  (11 other events, 27.9 us)
